TPU v7x, 256 devices: a 4x2x16 block of a 4x16x16 slice. The times are simulated.
256 devices in a mesh: grp: 2 (over y), ep: 32 (over z, core), tp: 4 (over x).
Axes of the slice: x: 4, y: 2, z: 16, core: 2. Of those that a mesh axis runs over, the one named last changes fastest.
The devices are a block of a 4x16x16 slice.
Arguments:
- query_vectors: bfloat16 [32768, 2048], P(('grp', 'ep'), 'tp'), parts along dimension 0, may hold values from -6 to 6
- attend_lookup_vectors: bfloat16 [32768, 2048], P(('grp', 'ep'), 'tp'), parts along dimension 0, may hold values from -6 to 6
- attend_content_vectors: bfloat16 [32768, 2048], P(('grp', 'ep'), 'tp'), parts along dimension 0, may hold values from -6 to 6
- forget_speed_dependent: bfloat16 [32768, 2048], P(('grp', 'ep'), 'tp'), parts along dimension 0, may hold values from -3 to 3
- amend_speed_dependent: bfloat16 [32768, 2048], P(('grp', 'ep'), 'tp'), parts along dimension 0, may hold values from -6 to 6
- result_switch_preactivation: bfloat16 [32768, 2048], P(('grp', 'ep'), 'tp'), parts along dimension 0, may hold values from -6 to 6
- feature_forget_baseline: float32 [2048], P('tp'), may hold values from -13 to -3
- amend_speed_baseline: float32 [2048], P('tp'), may hold values from -9 to 3
- sudden_forget_extra: float32 [32768, 32], P(('grp', 'ep'), 'tp'), parts along dimension 0, may hold values from -1 to 0
- group_scaling_factor: float32 [2048], P('tp'), may hold values from 0.1 to 1.9
- result_mapping_matrix: bfloat16 [2048, 2048], P('tp'), may hold values from -0.125 to 0.125
- specialist_tokens_activations: bfloat16 [32768, 2048], P(('grp', 'ep', 'tp')), parts along dimension 0, may hold values from -6 to 6
- specialist_scaling_factor: float32 [2048], replicated, may hold values from 0.1 to 1.9
- selected_specialists: int32 [32768, 2], P(('grp', 'ep', 'tp')), parts along dimension 0, may hold values from 0 to 31, all different within a row; in each aligned block of 128 rows (0 to 127, 128 to 255, ...) at most 12 rows name the same one
- selection_mixing_factors: float32 [32768, 2], P(('grp', 'ep', 'tp')), parts along dimension 0, may hold values from 0.3 to 1.5
- dispatched_switch_matrix: bfloat16 [32, 2048, 1024], P('ep', None, 'tp'), may hold values from -0.125 to 0.125
- dispatched_raising_matrix: bfloat16 [32, 2048, 1024], P('ep', None, 'tp'), may hold values from -0.125 to 0.125
- dispatched_lowering_matrix: bfloat16 [32, 1024, 2048], P('ep', 'tp'), may hold values from -0.1875 to 0.1875
- common_switch_matrix: bfloat16 [2048, 512], P(None, 'tp'), may hold values from -0.125 to 0.125
- common_raising_matrix: bfloat16 [2048, 512], P(None, 'tp'), may hold values from -0.125 to 0.125
- common_lowering_matrix: bfloat16 [512, 2048], P('tp'), may hold values from -0.25 to 0.25
Outputs:
- attend_result_matrix: bfloat16 [32768, 2048], P(('grp', 'ep', 'tp')), parts along dimension 0
- moe_out: bfloat16 [32768, 2048], P(('grp', 'ep', 'tp')), parts along dimension 0
There are 2 independent parts, one for each index of `grp`. A program takes and returns all parts, laid end to end along the dimension named above; an argument that names none is the same for every part. Nothing has to cross between parts.
Inputs may be any that keep to these rules, and one draw needn't show every extreme that they name: `selected_specialists`: each row names 2 different experts. Among the rows of one device no expert is named more than 12 times, and in every draw some device names some expert exactly 12 times.
All inputs are finite; a program needn't handle non-finite values.
Results may differ from a plain program's by a relative error of at most 0.023.
Values may be sent and summed in bfloat16 or wider, within the bound.
A program may use at most 128 MiB of HBM per device.

v0:
```python
import math

import jax
import jax.numpy as jnp
from jax import lax
from jax.sharding import PartitionSpec as P


def carried_in(shard, axis, combine, identity):
    count, position = (lax.axis_size(axis), lax.axis_index(axis))
    everything = jax.tree.map(
        lambda part, kind: lax.all_gather(part.astype(kind), axis),
        shard,
        (jnp.bfloat16, jnp.bfloat16),
    )
    start = jax.tree.map(
        lambda part, zero: jnp.broadcast_to(jnp.asarray(zero, part.dtype), part.shape),
        shard,
        identity,
    )

    def step(k, before):
        reached = k < position
        new = combine(
            before, jax.tree.map(lambda part, own: part[k].astype(own.dtype), everything, shard)
        )
        return jax.tree.map(lambda a, b: jnp.where(reached, a, b), new, before)

    return lax.fori_loop(0, count, step, start)


def masked_pair(left_side, right_side, pair_mask):
    product = jnp.einsum("shk,jhk->hsj", left_side, right_side)
    return jnp.where(pair_mask[None], product, 0.0)


def block_form(memory, inputs):
    recept_span, decay_span, write_span, value_span, unit_span, erase_span = inputs
    span_len = recept_span.shape[0]
    decay_cum = jnp.cumsum(decay_span, axis=0)
    decay_prev = decay_cum - decay_span
    middle = decay_cum[span_len // 2]
    erase_dir = -unit_span
    left_erase = erase_dir * jnp.exp(decay_prev - middle)
    left_read = recept_span * jnp.exp(decay_cum - middle)
    right_erase = erase_span * jnp.exp(middle - decay_cum)
    right_write = write_span * jnp.exp(middle - decay_cum)
    positions = jnp.arange(span_len)
    strict = positions[:, None] > positions[None, :]
    inclusive = positions[:, None] >= positions[None, :]
    erase_erase = masked_pair(left_erase, right_erase, strict)
    erase_write = masked_pair(left_erase, right_write, strict)
    read_erase = masked_pair(left_read, right_erase, inclusive)
    read_write = masked_pair(left_read, right_write, inclusive)
    value_pad = jnp.concatenate([value_span, jnp.zeros_like(value_span)], axis=2)
    solve_rhs = jnp.einsum("shk,hrk->hsr", erase_dir * jnp.exp(decay_prev), memory)
    solve_rhs = solve_rhs + jnp.einsum("hsj,jhr->hsr", erase_write, value_pad)
    identity = jnp.eye(span_len, dtype=jnp.float32)
    updates = jax.scipy.linalg.solve_triangular(
        identity[None] - erase_erase, solve_rhs, lower=True, unit_diagonal=True
    )
    outputs = jnp.einsum("shk,hrk->hsr", recept_span * jnp.exp(decay_cum), memory)
    outputs = outputs + jnp.einsum("hsj,hjr->hsr", read_erase, updates)
    outputs = outputs + jnp.einsum("hsj,jhr->hsr", read_write, value_pad)
    tail_decay = jnp.exp(decay_cum[-1][None] - decay_cum)
    memory = memory * jnp.exp(decay_cum[-1])[:, None, :]
    memory = memory + jnp.einsum("hjr,jhk->hrk", updates, erase_span * tail_decay)
    memory = memory + jnp.einsum("jhr,jhk->hrk", value_pad, write_span * tail_decay)
    return (memory, outputs)


def chain_pair(earlier_part, later_part):
    joined_map = jnp.einsum("hij,hjk->hik", earlier_part[0], later_part[0])
    joined_add = jnp.einsum("hij,hjk->hik", earlier_part[1], later_part[0]) + later_part[1]
    return (joined_map, joined_add)


def mixer_half(
    query_vectors,
    attend_lookup_vectors,
    attend_content_vectors,
    forget_speed_dependent,
    amend_speed_dependent,
    result_switch_preactivation,
    feature_forget_baseline,
    amend_speed_baseline,
    sudden_forget_extra,
    group_scaling_factor,
):
    tokens, mix_width = query_vectors.shape
    attend_group_total = sudden_forget_extra.shape[1]
    head_size = mix_width // attend_group_total

    def split_among_groups(array_in):
        return array_in.astype(jnp.float32).reshape(tokens, attend_group_total, head_size)

    forget_exponent_log = (
        -jnp.exp(
            feature_forget_baseline.reshape(attend_group_total, head_size)
            + split_among_groups(forget_speed_dependent)
        )
        + sudden_forget_extra[:, :, None]
    )
    learn_rate = jax.nn.sigmoid(
        amend_speed_baseline.reshape(attend_group_total, head_size)
        + split_among_groups(amend_speed_dependent)
    )
    key_heads = split_among_groups(attend_lookup_vectors)
    unit_key = key_heads * lax.rsqrt(jnp.sum(key_heads * key_heads, -1, keepdims=True) + 1e-06)
    span_len = math.gcd(tokens, 64)
    span_count = tokens // span_len

    def by_span(array_in):
        return array_in.reshape(span_count, span_len, attend_group_total, head_size)

    eye_heads = jnp.broadcast_to(
        jnp.eye(head_size, dtype=jnp.float32), (attend_group_total, head_size, head_size)
    )
    zero_heads = jnp.zeros((attend_group_total, head_size, head_size), jnp.float32)
    memory_zero = jnp.concatenate([zero_heads, eye_heads], axis=1)
    memory_end, outputs = lax.scan(
        block_form,
        memory_zero,
        (
            by_span(split_among_groups(query_vectors)),
            by_span(forget_exponent_log),
            by_span(key_heads * learn_rate),
            by_span(split_among_groups(attend_content_vectors)),
            by_span(unit_key),
            by_span(unit_key * learn_rate),
        ),
    )
    carried = memory_end[:, head_size:, :]
    offset = memory_end[:, :head_size, :]
    prefix = carried_in((carried, offset), "ep", chain_pair, (eye_heads, zero_heads))
    start_state = prefix[1]
    flat_out = outputs.transpose(0, 2, 1, 3).reshape(tokens, attend_group_total, 2 * head_size)
    head_out = flat_out[:, :, :head_size] + jnp.einsum(
        "thk,hvk->thv", flat_out[:, :, head_size:], start_state
    )
    head_mean = jnp.mean(head_out, -1, keepdims=True)
    centered = head_out - head_mean
    head_var = jnp.mean(centered * centered, -1, keepdims=True)
    normed = (
        centered
        * lax.rsqrt(head_var + 0.00064)
        * group_scaling_factor.reshape(attend_group_total, head_size)
    )
    mixed_rows = (normed * jax.nn.sigmoid(split_among_groups(result_switch_preactivation))).reshape(
        tokens, mix_width
    )
    return mixed_rows.astype(jnp.bfloat16)


def swiglu_rows(rows, gate_w, up_w):
    gate_vals = jnp.dot(rows, gate_w, preferred_element_type=jnp.float32)
    up_vals = jnp.dot(rows, up_w, preferred_element_type=jnp.float32)
    return (jax.nn.silu(gate_vals) * up_vals).astype(jnp.bfloat16)


def on_device(
    query_vectors,
    attend_lookup_vectors,
    attend_content_vectors,
    forget_speed_dependent,
    amend_speed_dependent,
    result_switch_preactivation,
    feature_forget_baseline,
    amend_speed_baseline,
    sudden_forget_extra,
    group_scaling_factor,
    result_mapping_matrix,
    specialist_tokens_activations,
    specialist_scaling_factor,
    selected_specialists,
    selection_mixing_factors,
    dispatched_switch_matrix,
    dispatched_raising_matrix,
    dispatched_lowering_matrix,
    common_switch_matrix,
    common_raising_matrix,
    common_lowering_matrix,
):
    mixed_rows = mixer_half(
        query_vectors,
        attend_lookup_vectors,
        attend_content_vectors,
        forget_speed_dependent,
        amend_speed_dependent,
        result_switch_preactivation,
        feature_forget_baseline,
        amend_speed_baseline,
        sudden_forget_extra,
        group_scaling_factor,
    )
    floats = specialist_tokens_activations.astype(jnp.float32)
    normed = (
        floats
        * lax.rsqrt(jnp.mean(floats * floats, -1, keepdims=True) + 1e-06)
        * specialist_scaling_factor
    )
    normed = normed.astype(jnp.bfloat16)
    tok_rows, top_count = selected_specialists.shape
    model_width = specialist_tokens_activations.shape[1]
    experts = lax.axis_size("ep")
    tp_size = lax.axis_size("tp")
    capacity = 3 * tok_rows * top_count // (2 * experts)
    flat_ids = selected_specialists.reshape(-1)
    one_hot = (flat_ids[:, None] == jnp.arange(experts, dtype=jnp.int32)[None, :]).astype(jnp.int32)
    slot_rank = jnp.sum((jnp.cumsum(one_hot, axis=0) - 1) * one_hot, axis=1)
    position = flat_ids * capacity + slot_rank
    placing = position[:, None] == jnp.arange(experts * capacity, dtype=jnp.int32)[None, :]
    placing = jnp.sum(
        placing.astype(jnp.bfloat16).reshape(tok_rows, top_count, experts * capacity), axis=1
    )
    outgoing = jnp.einsum("te,td->ed", placing, normed, preferred_element_type=jnp.float32).astype(
        jnp.bfloat16
    )
    gate_w = dispatched_switch_matrix[0]
    up_w = dispatched_raising_matrix[0]
    down_w = dispatched_lowering_matrix[0]
    received = lax.all_to_all(
        outgoing.reshape(experts, capacity, model_width),
        "ep",
        split_axis=0,
        concat_axis=0,
        tiled=True,
    )
    local_rows = experts * capacity
    hidden = swiglu_rows(
        lax.all_gather(received.reshape(local_rows, model_width), "tp", axis=0, tiled=True),
        gate_w,
        up_w,
    )
    summed = lax.psum_scatter(
        jnp.dot(hidden, down_w, preferred_element_type=jnp.float32).astype(jnp.bfloat16),
        "tp",
        scatter_dimension=0,
        tiled=True,
    )
    expert_out = lax.all_to_all(
        summed.reshape(experts, capacity, model_width),
        "ep",
        split_axis=0,
        concat_axis=0,
        tiled=True,
    ).reshape(experts * capacity, model_width)
    picked = jnp.take(expert_out, position, axis=0).astype(jnp.float32)
    routed = jnp.sum(
        (picked * selection_mixing_factors.reshape(-1)[:, None]).reshape(
            tok_rows, top_count, model_width
        ),
        axis=1,
    )
    shared_hidden = swiglu_rows(
        lax.all_gather(normed, "tp", axis=0, tiled=True),
        common_switch_matrix,
        common_raising_matrix,
    )
    mixer_rows = mixed_rows.shape[0] // tp_size
    per_device = mixer_rows + tok_rows
    first_device = jnp.int32(0) // per_device
    blocks = []
    for turn_id in range(per_device * lax.axis_size("tp") // per_device):
        device = first_device + turn_id
        blocks.append(
            jnp.dot(
                lax.dynamic_slice_in_dim(mixed_rows, device * mixer_rows, mixer_rows, 0),
                result_mapping_matrix,
                preferred_element_type=jnp.float32,
            )
        )
        blocks.append(
            jnp.dot(
                lax.dynamic_slice_in_dim(shared_hidden, device * tok_rows, tok_rows, 0),
                common_lowering_matrix,
                preferred_element_type=jnp.float32,
            )
        )
    joined = lax.psum_scatter(
        jnp.concatenate(blocks, axis=0).astype(jnp.bfloat16), "tp", scatter_dimension=0, tiled=True
    ).astype(jnp.float32)
    attend_result_matrix = joined[:mixer_rows]
    shared_sum = joined[mixer_rows:]
    moe_out = (routed + shared_sum).astype(jnp.bfloat16)
    return (attend_result_matrix.astype(jnp.bfloat16), moe_out)


def solution(mesh):
    placed = (
        P(("grp", "ep"), "tp"),
        P(("grp", "ep"), "tp"),
        P(("grp", "ep"), "tp"),
        P(("grp", "ep"), "tp"),
        P(("grp", "ep"), "tp"),
        P(("grp", "ep"), "tp"),
        P("tp"),
        P("tp"),
        P(("grp", "ep"), "tp"),
        P("tp"),
        P("tp", None),
        P(("grp", "ep", "tp"), None),
        P(),
        P(("grp", "ep", "tp"), None),
        P(("grp", "ep", "tp"), None),
        P("ep", None, "tp"),
        P("ep", None, "tp"),
        P("ep", "tp", None),
        P(None, "tp"),
        P(None, "tp"),
        P("tp", None),
    )
    return jax.shard_map(
        on_device,
        mesh=mesh,
        in_specs=placed,
        out_specs=(P(("grp", "ep", "tp"), None), P(("grp", "ep", "tp"), None)),
        check_vma=False,
    )
```

profile of v0, /device:TPU:33, one launch (start us, length us, event | category | flops | bytes accessed | tf_op | source)
XLA Modules:
  0.0 947.2 jit_solution(15160833496766794190)
XLA Ops:
  18.2 25.6 %all-to-all-start = ((bf16[32,12,2048]{2,1,0:T(8,128)(2,1)}), bf16[32,12,2048]{2,1,0:T(8,128)(2,1)}, u32[]{:S(2)}, u32[]{:S(2)}) async-start(bf16[32,12,2048]{2,1,0:T(8,128)(2,1)} %reshape.237), calls=%async_computation.1 | async-start | bytes 4194304 | tf_op jit(solution)/shard_map/all_to_all | solution.py:222
  46.8 3.7 copy.143
  59.9 5.8 fusion.85
  65.7 76.9 %all-to-all-done = bf16[32,12,2048]{2,1,0:T(8,128)(2,1)} async-done(((bf16[32,12,2048]{2,1,0:T(8,128)(2,1)}), bf16[32,12,2048]{2,1,0:T(8,128)(2,1)}, u32[]{:S(2)}, u32[]{:S(2)}) %all-to-all-start) | async-done | bytes 1572896 | tf_op jit(solution)/shard_map/all_to_all | solution.py:222
  146.3 443.8 %while.26 = (s32[]{:T(128)}, f32[8,128,64]{1,2,0:T(8,128)S(1)}, f32[8,8,64,128]{3,1,2,0:T(8,128)}, f32[8,64,8,64]{3,2,1,0:T(8,128)}, f32[8,64,8,64]{3,2,1,0:T(8,...) while((s32[]{:T(128)}, f32[8,128,64]{1,2,0:T(8,128)S(1)}, ...), condition=%wide.region_3.4_spmd, body=%wide.region_1.3_spmd.sunk | while | flops 129265728 | bytes 8965825 | solution.py:121
  150.5 40.0 %custom-call.11 = f32[8,1,64,64]{2,3,1,0:T(8,128)} custom-call(f32[8,1,64,64]{3,2,1,0:T(8,128)S(1)} %fusion.186), custom_call_target="InvertDiagBlocksLowerTriangular" | custom-call | tf_op jit(solution)/shard_map/while/body/eval_jaxpr/jit(_solve_triangular)/vmap()/triangular_solve | solution.py:59
  206.0 40.0 %custom-call.11 = f32[8,1,64,64]{2,3,1,0:T(8,128)} custom-call(f32[8,1,64,64]{3,2,1,0:T(8,128)S(1)} %fusion.186), custom_call_target="InvertDiagBlocksLowerTriangular" | custom-call | tf_op jit(solution)/shard_map/while/body/eval_jaxpr/jit(_solve_triangular)/vmap()/triangular_solve | solution.py:59
  261.5 40.0 %custom-call.11 = f32[8,1,64,64]{2,3,1,0:T(8,128)} custom-call(f32[8,1,64,64]{3,2,1,0:T(8,128)S(1)} %fusion.186), custom_call_target="InvertDiagBlocksLowerTriangular" | custom-call | tf_op jit(solution)/shard_map/while/body/eval_jaxpr/jit(_solve_triangular)/vmap()/triangular_solve | solution.py:59
  317.0 40.0 %custom-call.11 = f32[8,1,64,64]{2,3,1,0:T(8,128)} custom-call(f32[8,1,64,64]{3,2,1,0:T(8,128)S(1)} %fusion.186), custom_call_target="InvertDiagBlocksLowerTriangular" | custom-call | tf_op jit(solution)/shard_map/while/body/eval_jaxpr/jit(_solve_triangular)/vmap()/triangular_solve | solution.py:59
  372.4 40.0 %custom-call.11 = f32[8,1,64,64]{2,3,1,0:T(8,128)} custom-call(f32[8,1,64,64]{3,2,1,0:T(8,128)S(1)} %fusion.186), custom_call_target="InvertDiagBlocksLowerTriangular" | custom-call | tf_op jit(solution)/shard_map/while/body/eval_jaxpr/jit(_solve_triangular)/vmap()/triangular_solve | solution.py:59
  427.9 40.0 %custom-call.11 = f32[8,1,64,64]{2,3,1,0:T(8,128)} custom-call(f32[8,1,64,64]{3,2,1,0:T(8,128)S(1)} %fusion.186), custom_call_target="InvertDiagBlocksLowerTriangular" | custom-call | tf_op jit(solution)/shard_map/while/body/eval_jaxpr/jit(_solve_triangular)/vmap()/triangular_solve | solution.py:59
  483.4 40.0 %custom-call.11 = f32[8,1,64,64]{2,3,1,0:T(8,128)} custom-call(f32[8,1,64,64]{3,2,1,0:T(8,128)S(1)} %fusion.186), custom_call_target="InvertDiagBlocksLowerTriangular" | custom-call | tf_op jit(solution)/shard_map/while/body/eval_jaxpr/jit(_solve_triangular)/vmap()/triangular_solve | solution.py:59
  538.9 40.0 %custom-call.11 = f32[8,1,64,64]{2,3,1,0:T(8,128)} custom-call(f32[8,1,64,64]{3,2,1,0:T(8,128)S(1)} %fusion.186), custom_call_target="InvertDiagBlocksLowerTriangular" | custom-call | tf_op jit(solution)/shard_map/while/body/eval_jaxpr/jit(_solve_triangular)/vmap()/triangular_solve | solution.py:59
  606.0 6.1 fusion.80
  612.0 12.9 %convolution_convert_fusion = bf16[1536,2048]{1,0:T(8,128)(2,1)} fusion(bf16[1536,2048]{1,0:T(8,128)(2,1)} %all-gather.9.cloned.1.call-done, f32[1536,256]{1,0:T(8,128)} %fusion.80, bf16[1,256,2048]{2,1,0:T(8,128)(2,1)} %param.42, bf16[1,2048,256]{2,1,0:T(8,128)(2,1)} %param.41), kind=kOutput, calls=%fused_computation.85 | convolution fusion | flops 3226730496 | bytes 16252928 | tf_op jit(solution)/shard_map/dot_general | solution.py:236
  625.3 32.4 %all-gather.11.cloned.1.call-done = bf16[256,64,64]{2,1,0:T(8,128)(2,1)} async-done(((bf16[8,64,64]{2,1,0:T(8,128)(2,1)}), bf16[256,64,64]{2,1,0:T(8,128)(2,1)}) %all-gather.11.cloned.1.call-update) | async-done | bytes 2097168 | tf_op jit(solution)/shard_map/all_gather | solution.py:12
  657.7 71.4 %all-gather.13.cloned.1.call-done = bf16[256,64,64]{2,1,0:T(8,128)(2,1)} async-done(((bf16[8,64,64]{2,1,0:T(8,128)(2,1)}), bf16[256,64,64]{2,1,0:T(8,128)(2,1)}) %all-gather.13.cloned.1.call-update) | async-done | bytes 2097168 | tf_op jit(solution)/shard_map/all_gather | solution.py:12
  729.1 72.3 %while.27 = (s32[]{:T(128)}, bf16[8,64,64]{1,2,0:T(8,128)(2,1)S(1)}, s32[]{:T(128)}, bf16[32,8,64,64]{3,2,1,0:T(8,128)(2,1)}, bf16[32,8,64,64]{3,2,1,0:T(8,128)(2,1)}, /*index=5*/s32[]{:T(128)}, s32[]{:T(128)}) while((s32[]{:T(128)}, bf16[8,64,64]{1,2,0:T(8,128)(2,1)S(1)}, s32[]{:T(128)}, bf16[32,8,64,64]{3,2,1,0:T(8,128)(2,1)}, ...), condition=%wide.region_5.6_spmd.clone, body=%wide.region_4.5_spmd.clone.sunk | while | flops 4358148 | bytes 985187 | solution.py:29
  817.1 8.9 all-to-all-start.1
  826.6 36.8 %reduce-scatter.3.cloned.1.call-done = bf16[256,2048]{1,0:T(8,128)(2,1)} async-done(((bf16[1024,2048]{1,0:T(8,128)(2,1)}), bf16[256,2048]{1,0:T(8,128)(2,1)}) %reduce-scatter.3.cloned.1.call-update) | async-done | bytes 1048592 | tf_op jit(solution)/shard_map/reduce_scatter | solution.py:280
  865.2 59.5 %all-to-all-done.1 = bf16[32,12,2048]{2,1,0:T(8,128)(2,1)} async-done(((bf16[32,12,2048]{2,1,0:T(8,128)(2,1)}), bf16[32,12,2048]{2,1,0:T(8,128)(2,1)}, u32[]{:S(2)}, u32[]{:S(2)}) %all-to-all-start.1) | async-done | bytes 1572896 | tf_op jit(solution)/shard_map/all_to_all | solution.py:241
  924.7 3.7 reshape.240
  928.4 4.0 gather_fusion
  933.9 5.5 multiply_reduce_fusion
  (455 shorter events, 257.5 us)
Async XLA Ops:
  7.2 796.7 %copy-start = (bf16[512,2048]{1,0:T(8,128)(2,1)S(1)}, bf16[512,2048]{1,0:T(8,128)(2,1)}, u32[]{:S(2)}) copy-start(bf16[512,2048]{1,0:T(8,128)(2,1)} %param.35) | copy-start | bytes 6291460
  12.9 5.4 copy-start.5
  18.2 26.5 %copy-start.11 = (bf16[512,512]{1,0:T(8,128)(2,1)S(1)}, bf16[512,512]{1,0:T(8,128)(2,1)}, u32[]{:S(2)}) copy-start(bf16[512,512]{1,0:T(8,128)(2,1)} %param.26) | copy-start | bytes 1572868
  18.2 124.3 %all-to-all-start = ((bf16[32,12,2048]{2,1,0:T(8,128)(2,1)}), bf16[32,12,2048]{2,1,0:T(8,128)(2,1)}, u32[]{:S(2)}, u32[]{:S(2)}) async-start(bf16[32,12,2048]{2,1,0:T(8,128)(2,1)} %reshape.237), calls=%async_computation.1 | async-start | bytes 4194304 | tf_op jit(solution)/shard_map/all_to_all | solution.py:222
  43.9 558.2 %all-gather.7.cloned.1.call-start = ((), (), s32[]{:S(2)}) async-start(), calls=%async_computation.4 | async-start | bytes 2621440 | tf_op jit(solution)/shard_map/all_gather | solution.py:256
  44.6 561.3 %all-gather.9.cloned.1.call-start = ((), (), s32[]{:S(2)}) async-start(), calls=%async_computation.6 | async-start | bytes 7864320 | tf_op jit(solution)/shard_map/all_gather | solution.py:231
  50.8 4.5 copy-start.13
  146.2 511.4 %all-gather.11.cloned.1.call-start = ((), (), s32[]{:S(2)}) async-start(), calls=%async_computation.8 | async-start | bytes 4325376 | tf_op jit(solution)/shard_map/all_gather | solution.py:12
  194.4 7.2 copy-start.3
  249.9 7.2 copy-start.3
  305.4 7.2 copy-start.3
  360.8 7.2 copy-start.3
  416.3 7.2 copy-start.3
  471.8 7.2 copy-start.3
  527.2 7.2 copy-start.3
  582.7 7.1 copy-start.3
  591.1 138.0 %all-gather.13.cloned.1.call-start = ((), (), s32[]{:S(2)}) async-start(), calls=%async_computation.9 | async-start | bytes 4325376 | tf_op jit(solution)/shard_map/all_gather | solution.py:12
  591.7 221.7 %reduce-scatter.5.cloned.1.call-start = ((), (), s32[]{:S(2)}) async-start(), calls=%async_computation.7 | async-start | bytes 7864320 | tf_op jit(solution)/shard_map/reduce_scatter | solution.py:235
  597.1 4.9 copy-start.17
  625.0 238.3 %reduce-scatter.3.cloned.1.call-start = ((), (), s32[]{:S(2)}) async-start(), calls=%async_computation.5 | async-start | bytes 5242880 | tf_op jit(solution)/shard_map/reduce_scatter | solution.py:280
  817.1 8.9 copy-start.14
  817.1 9.3 copy-start.18
  817.1 107.6 %all-to-all-start.1 = ((bf16[32,12,2048]{2,1,0:T(8,128)(2,1)}), bf16[32,12,2048]{2,1,0:T(8,128)(2,1)}, u32[]{:S(2)}, u32[]{:S(2)}) async-start(bf16[32,12,2048]{2,1,0:T(8,128)(2,1)} %reshape.239), calls=%async_computation.3 | async-start | bytes 4194304 | tf_op jit(solution)/shard_map/all_to_all | solution.py:241
  933.9 5.6 copy-start.8
  (25 other events, 33.6 us)
Sparse Core Ops, SparseCore 0:
  47.1 38.1 all-gather.6
  146.4 65.9 all-gather.8
  591.2 66.3 all-gather.10
  659.9 69.0 all-gather.12
  731.5 66.8 reduce-scatter.4
  813.6 49.7 reduce-scatter.2
where the time goes:
time: 951 us; the launch traced here: 947 us
  other arithmetic  366 us (38%)
  waiting for transfers between devices  278 us (29%)
  matrix products  142 us (15%)
  local copies, waits for them, and re-layouts  108 us (11%)
  starting transfers between devices  35.3 us (4%)
  between operations  14.5 us (2%)
    another operation x16, other arithmetic, block_form(): jax.scipy.linalg.solve_triangular(identity[None] - erase_erase, solve_rhs...  320 us
    all_gather x2, waiting for transfers between devices, carried_in(): lax.all_gather(part.astype(kind), axis)  104 us
    all_to_all x1, waiting for transfers between devices, on_device(): lax.all_to_all(outgoing.reshape(experts, capacity, model_width), 'ep', sp...  76.9 us
    all_to_all x1, waiting for transfers between devices, on_device(): lax.all_to_all(summed.reshape(experts, capacity, model_width), 'ep', spli...  59.5 us
    dot_general x32, matrix products, chain_pair(): jnp.einsum('hij,hjk->hik', earlier_part[1], later_part[0]) + later_part[1]  37 us
    reduce_scatter x1, waiting for transfers between devices, on_device(): lax.psum_scatter(jnp.concatenate(blocks, axis=0).astype(jnp.bfloat16), 't...  36.8 us
    dynamic_slice x64, local copies, waits for them, and re-layouts, step(): part[k].astype(own.dtype)  33.5 us
    all_to_all x1, starting transfers between devices, on_device(): lax.all_to_all(outgoing.reshape(experts, capacity, model_width), 'ep', sp...  25.6 us
  transfers between devices with their start and end apart: 8, of which 5 were waited for; matrix products, arithmetic and copies ran while one was open for 62% of the time, Pallas kernels for 0%

commit v1 on v0

v1 whole, which is shorter than its diff:
```python
import functools

import jax
import jax.numpy as jnp
from jax import lax
from jax.experimental import pallas as pl
from jax.experimental.pallas import tpu as pltpu
from jax.sharding import PartitionSpec as P

F32 = jnp.float32
BF16 = jnp.bfloat16
SPAN = 64
MESH = pl.DeviceIdType.MESH


def dot(a, b):
    return jnp.dot(a, b, preferred_element_type=F32)


def dot_nt(a, b):
    return lax.dot_general(a, b, (((1,), (1,)), ((), ())), preferred_element_type=F32)


def dot_tn(a, b):
    return lax.dot_general(a, b, (((0,), (0,)), ((), ())), preferred_element_type=F32)


def split(x, parts):
    out = []
    for _ in range(parts - 1):
        out.append(x.astype(BF16))
        x = x - out[-1].astype(F32)
    out.append(x.astype(BF16))
    return out


def iota(shape, dim):
    return lax.broadcasted_iota(jnp.int32, shape, dim)


def local_mixer(
    q_ref, k_ref, v_ref, f_ref, a_ref, fb_ref, ab_ref, x_ref, omap_ref, oloc_ref, pay_ref
):
    rows, lanes = q_ref.shape
    half = lanes // 2
    spans = rows // SPAN
    groups = x_ref.shape[1]
    pair = pl.program_id(0)
    low = iota((SPAN, lanes), 1) < half
    col = jnp.where(low, iota((SPAN, lanes), 1), iota((SPAN, lanes), 1) - half)
    row = iota((SPAN, lanes), 0)
    strict = row > col
    inclusive = row >= col
    tri = (iota((SPAN, SPAN), 0) >= iota((SPAN, SPAN), 1)).astype(BF16)
    tri3 = jnp.concatenate([tri] * 3, axis=1)
    same = ((iota((lanes, lanes), 0) < half) == (iota((lanes, lanes), 1) < half)).astype(BF16)
    same2 = jnp.concatenate([same] * 2, axis=0)
    spread = (
        iota((groups, lanes), 0) == 2 * pair + (iota((groups, lanes), 1) >= half).astype(jnp.int32)
    ).astype(BF16)
    spread3 = jnp.concatenate([spread] * 3, axis=0)
    below = iota((lanes, lanes), 0) < half
    left = iota((lanes, lanes), 1) < half

    def stack(x):
        return jnp.concatenate([jnp.where(low, x, 0.0), jnp.where(low, 0.0, x)], axis=0).astype(
            BF16
        )

    fb = fb_ref[...]
    ab = ab_ref[...]
    extra = dot(jnp.concatenate(split(x_ref[...], 3), axis=1), spread3)

    spans_in = []
    for c in range(spans):
        at = slice(c * SPAN, (c + 1) * SPAN)
        decay = -jnp.exp(fb + f_ref[at, :].astype(F32)) + extra[at, :]
        rate = jax.nn.sigmoid(ab + a_ref[at, :].astype(F32))
        key = k_ref[at, :].astype(F32)
        sq = dot(jnp.concatenate(split(key * key, 2), axis=1), same2)
        unit = key * lax.rsqrt(sq + 1e-06)
        cum = dot(tri3, jnp.concatenate(split(decay, 3), axis=0))
        mid = cum[SPAN // 2 : SPAN // 2 + 1, :]
        last = cum[SPAN - 1 : SPAN, :]
        left_erase = -unit * jnp.exp(cum - decay - mid)
        left_read = q_ref[at, :].astype(F32) * jnp.exp(cum - mid)
        right = jnp.exp(mid - cum) * rate
        right_erase = unit * right
        right_write = key * right
        grow = jnp.exp(mid)
        tail = jnp.exp(last - mid)
        lefts = jnp.concatenate([left_erase, left_read], axis=0).astype(BF16)
        rights = jnp.concatenate([stack(right_erase), stack(right_write)], axis=0)
        pairs = dot_nt(lefts, rights)
        a_mat = jnp.where(strict, pairs[:SPAN, :lanes], 0.0)
        erase_write = jnp.where(strict, pairs[:SPAN, lanes:], 0.0)
        read_erase = jnp.where(inclusive, pairs[SPAN:, :lanes], 0.0)
        read_write = jnp.where(inclusive, pairs[SPAN:, lanes:], 0.0)
        value = v_ref[at, :].astype(F32)
        writes = dot(
            jnp.concatenate([erase_write, read_write], axis=0).astype(BF16), stack(value)
        )
        ends = jnp.concatenate([right_erase * tail, right_write * tail], axis=0).astype(BF16)
        spans_in.append(
            dict(
                a=a_mat,
                first=stack(left_erase * grow),
                read=left_read * grow,
                re=read_erase.astype(BF16),
                ew=stack(writes[:SPAN]),
                rw=writes[SPAN:],
                ends=ends,
                value=v_ref[at, :],
                last=jnp.exp(last),
            )
        )

    eye = (row == col).astype(F32)
    block = 1
    inverse = None
    while block < SPAN:
        in_block = (row // (2 * block) == col // (2 * block)) & (
            (row // block) % 2 == 1
        ) & ((col // block) % 2 == 0)
        steps = [jnp.where(in_block, s["a"], 0.0) for s in spans_in]
        if inverse is None:
            inverse = [eye + step for step in steps]
        else:
            inner = [
                dot(step.astype(BF16), stack(x)) for step, x in zip(steps, inverse)
            ]
            inverse = [x + dot(x.astype(BF16), stack(y)) for x, y in zip(inverse, inner)]
        block *= 2

    state = jnp.concatenate([eye, jnp.zeros_like(eye)], axis=0)
    for c, s in enumerate(spans_in):
        at = slice(c * SPAN, (c + 1) * SPAN)
        solved = dot(inverse[c].astype(BF16), jnp.concatenate([s["first"], s["ew"]], axis=1))
        w, y = (solved[:, :lanes], solved[:, lanes:])
        seen = dot(s["re"], jnp.concatenate([stack(w), stack(y)], axis=1))
        read = s["read"] + seen[:, :lanes]
        added = s["rw"] + seen[:, lanes:]
        value = s["value"]
        erased = dot_tn(w.astype(BF16), s["ends"][:SPAN])
        erased = jnp.where(below == left, erased, 0.0).astype(BF16)
        offset = dot_tn(jnp.concatenate([y.astype(BF16), value], axis=0), s["ends"])
        offset = jnp.where(low, offset[:half], offset[half:])
        both = jnp.concatenate([stack(state[:SPAN]), stack(state[SPAN:])], axis=0)
        reads = dot_nt(read.astype(BF16), both)
        omap_ref[at, :] = reads[:, :lanes].astype(BF16)
        oloc_ref[at, :] = added + reads[:, lanes:]
        state = (
            state * s["last"]
            + dot(state.astype(BF16), erased)
            + jnp.concatenate([jnp.zeros_like(offset), offset], axis=0)
        )
    jump, offset = (state[:SPAN], state[SPAN:])
    quarter = SPAN // 4
    eighth = SPAN // 8
    half_low = low[: SPAN // 2]
    jump_turned = pltpu.roll(jump, half, 1)
    offset_turned = pltpu.roll(offset, half, 1)
    empty = jnp.zeros((eighth, lanes), F32)
    for h in range(2):
        top = (jump, jump_turned)[h][: SPAN // 2]
        bottom = (jump_turned, jump)[h][SPAN // 2 :]
        packed = jnp.where(half_low, top, bottom)
        for j in range(4):
            top = (offset, offset_turned)[h][j * quarter : j * quarter + eighth]
            bottom = (offset_turned, offset)[h][j * quarter + eighth : (j + 1) * quarter]
            piece = jnp.where(low[:eighth], top, bottom)
            pay_ref[4 * h + j] = jnp.concatenate([packed, piece, empty], axis=0).astype(BF16)


def run_local_mixer(q, k, v, f, a, fb, ab, extra):
    rows, width = q.shape
    groups = extra.shape[1]
    lanes = 2 * (width // groups)
    tall = pl.BlockSpec((rows, lanes), lambda i: (0, i))
    flat = pl.BlockSpec((1, lanes), lambda i: (0, i))
    return pl.pallas_call(
        local_mixer,
        grid=(width // lanes,),
        in_specs=[tall] * 5 + [flat] * 2 + [pl.BlockSpec((rows, groups), lambda i: (0, 0))],
        out_specs=(tall, tall, pl.BlockSpec((8, 48, lanes), lambda i: (i, 0, 0))),
        out_shape=(
            jax.ShapeDtypeStruct((rows, width), BF16),
            jax.ShapeDtypeStruct((rows, width), F32),
            jax.ShapeDtypeStruct((4 * groups, 48, lanes), BF16),
        ),
        compiler_params=pltpu.CompilerParams(vmem_limit_bytes=48 * 1024 * 1024),
        cost_estimate=pl.CostEstimate(
            flops=10_000_000_000, bytes_accessed=6_000_000, transcendentals=1_500_000
        ),
        name="local_mixer",
    )(q, k, v, f, a, fb.reshape(1, -1), ab.reshape(1, -1), extra)


def fold_states(pay_ref, out_ref, arrived, sent, send_sem, recv_sem, back_sem, home_sem, own_sem):
    count = pay_ref.shape[0]
    lanes = pay_ref.shape[2]
    half = lanes // 2
    me = lax.axis_index("ep")
    barrier = pltpu.get_barrier_semaphore()

    def greet(d, carry):
        pl.semaphore_signal(
            barrier, inc=1, device_id={"ep": lax.rem(me + d, count)}, device_id_type=MESH
        )
        return carry

    lax.fori_loop(1, count, greet, 0)
    pl.semaphore_wait(barrier, count - 1)

    def outward(d):
        to = lax.rem(me + d, count)
        return pltpu.make_async_remote_copy(
            src_ref=pay_ref.at[to],
            dst_ref=arrived.at[me],
            send_sem=send_sem.at[d],
            recv_sem=recv_sem.at[me],
            device_id={"ep": to},
            device_id_type=MESH,
        )

    def inward(e):
        return pltpu.make_async_remote_copy(
            src_ref=pay_ref.at[e],
            dst_ref=arrived.at[e],
            send_sem=send_sem.at[0],
            recv_sem=recv_sem.at[e],
            device_id={"ep": e},
            device_id_type=MESH,
        )

    def go(d, carry):
        outward(d).start()
        return carry

    lax.fori_loop(1, count, go, 0)
    own = pltpu.make_async_copy(pay_ref.at[me], arrived.at[me], own_sem.at[0])
    own.start()
    own.wait()

    def homeward(e):
        return pltpu.make_async_remote_copy(
            src_ref=sent.at[e],
            dst_ref=out_ref.at[me],
            send_sem=back_sem.at[e],
            recv_sem=home_sem.at[me],
            device_id={"ep": e},
            device_id_type=MESH,
        )

    low = iota((lanes // 4, lanes), 1) < half

    def step(e, state):
        sent[e] = state

        @pl.when(e != me)
        def _():
            inward(e).wait_recv()

        @pl.when((e > 0) & (e - 1 != me))
        def _():
            homeward(e - 1).start()

        block = arrived[e].astype(F32)
        jump, offset = (block[: lanes // 4], block[lanes // 4 : lanes // 4 + 8])
        turned = pltpu.roll(jump, half, 1)
        spread = jnp.concatenate(
            [
                jnp.where(low, jump, 0.0),
                jnp.where(low, turned, 0.0),
                jnp.where(low, 0.0, turned),
                jnp.where(low, 0.0, jump),
            ],
            axis=0,
        ).astype(BF16)
        moved = dot(jnp.concatenate(split(state, 2), axis=0), spread)
        return moved[:8] + moved[8:] + offset

    lax.fori_loop(0, count, step, jnp.zeros((8, lanes), F32))

    @pl.when(me != count - 1)
    def _():
        homeward(count - 1).start()

    own = pltpu.make_async_copy(sent.at[me], out_ref.at[me], own_sem.at[1])
    own.start()
    own.wait()

    def finish(d, carry):
        outward(d).wait_send()
        return carry

    lax.fori_loop(1, count, finish, 0)

    def drain(d, carry):
        e = lax.rem(me + d, count)
        homeward(e).wait_send()
        pltpu.make_async_remote_copy(
            src_ref=sent.at[e],
            dst_ref=out_ref.at[e],
            send_sem=back_sem.at[e],
            recv_sem=home_sem.at[e],
            device_id={"ep": e},
            device_id_type=MESH,
        ).wait_recv()
        return carry

    lax.fori_loop(1, count, drain, 0)


def run_fold_states(pay):
    count, _, lanes = pay.shape
    vmem = pl.BlockSpec(memory_space=pltpu.VMEM)
    return pl.pallas_call(
        fold_states,
        in_specs=[vmem],
        out_specs=vmem,
        out_shape=jax.ShapeDtypeStruct((count, 8, lanes), F32),
        scratch_shapes=[
            pltpu.VMEM(pay.shape, BF16),
            pltpu.VMEM((count, 8, lanes), F32),
            pltpu.SemaphoreType.DMA((count,)),
            pltpu.SemaphoreType.DMA((count,)),
            pltpu.SemaphoreType.DMA((count,)),
            pltpu.SemaphoreType.DMA((count,)),
            pltpu.SemaphoreType.DMA((2,)),
        ],
        compiler_params=pltpu.CompilerParams(
            collective_id=0, has_side_effects=True, vmem_limit_bytes=16 * 1024 * 1024
        ),
        cost_estimate=pl.CostEstimate(
            flops=20_000_000_000, bytes_accessed=3_000_000, transcendentals=0
        ),
        name="fold_states",
    )(pay)


def finish_mixer(omap_ref, oloc_ref, state_ref, gate_ref, gain_ref, out_ref):
    rows, lanes = omap_ref.shape
    half = lanes // 2
    low = iota((8, lanes), 1) < half
    zero = jnp.zeros((8, lanes), F32)
    tiles = []
    for h in range(2):
        for j in range(4):
            block = state_ref[4 * h + j]
            turned = pltpu.roll(block, half, 1)
            if h == 0:
                tiles += [jnp.where(low, block, zero), jnp.where(low, turned, zero)]
            else:
                tiles += [jnp.where(low, zero, turned), jnp.where(low, zero, block)]
    state = jnp.concatenate(tiles, axis=0).astype(BF16)
    same = jnp.where(
        (iota((lanes, lanes), 0) < half) == (iota((lanes, lanes), 1) < half), 1.0 / half, 0.0
    ).astype(BF16)
    same2 = jnp.concatenate([same] * 2, axis=0)
    head_out = oloc_ref[...] + dot_nt(omap_ref[...], state)
    mean = dot(jnp.concatenate(split(head_out, 2), axis=1), same2)
    centered = head_out - mean
    var = dot(jnp.concatenate(split(centered * centered, 2), axis=1), same2)
    normed = centered * lax.rsqrt(var + 0.00064) * gain_ref[...]
    out_ref[...] = (normed * jax.nn.sigmoid(gate_ref[...].astype(F32))).astype(BF16)


def run_finish_mixer(omap, oloc, states, gate, gain):
    rows, width = omap.shape
    lanes = states.shape[2]
    tall = pl.BlockSpec((rows, lanes), lambda i: (0, i))
    return pl.pallas_call(
        finish_mixer,
        grid=(width // lanes,),
        in_specs=[
            tall,
            tall,
            pl.BlockSpec((8, 8, lanes), lambda i: (i, 0, 0)),
            tall,
            pl.BlockSpec((1, lanes), lambda i: (0, i)),
        ],
        out_specs=tall,
        out_shape=jax.ShapeDtypeStruct((rows, width), BF16),
        compiler_params=pltpu.CompilerParams(vmem_limit_bytes=32 * 1024 * 1024),
        cost_estimate=pl.CostEstimate(
            flops=1_000_000_000, bytes_accessed=3_000_000, transcendentals=300_000
        ),
        name="finish_mixer",
    )(omap, oloc, states, gate, gain.reshape(1, -1))


def swiglu(rows, gate_w, up_w):
    return (jax.nn.silu(dot(rows, gate_w)) * dot(rows, up_w)).astype(BF16)


def on_device(
    query_vectors,
    attend_lookup_vectors,
    attend_content_vectors,
    forget_speed_dependent,
    amend_speed_dependent,
    result_switch_preactivation,
    feature_forget_baseline,
    amend_speed_baseline,
    sudden_forget_extra,
    group_scaling_factor,
    result_mapping_matrix,
    specialist_tokens_activations,
    specialist_scaling_factor,
    selected_specialists,
    selection_mixing_factors,
    dispatched_switch_matrix,
    dispatched_raising_matrix,
    dispatched_lowering_matrix,
    common_switch_matrix,
    common_raising_matrix,
    common_lowering_matrix,
):
    floats = specialist_tokens_activations.astype(F32)
    normed = (
        floats
        * lax.rsqrt(jnp.mean(floats * floats, -1, keepdims=True) + 1e-06)
        * specialist_scaling_factor
    ).astype(BF16)
    tok_rows, top_count = selected_specialists.shape
    model_width = specialist_tokens_activations.shape[1]
    experts = lax.axis_size("ep")
    tp_size = lax.axis_size("tp")
    capacity = 3 * tok_rows * top_count // (2 * experts)
    slots = experts * capacity
    gates = lax.all_gather(dispatched_switch_matrix[0], "tp")
    ups = lax.all_gather(dispatched_raising_matrix[0], "tp")
    downs = lax.all_gather(dispatched_lowering_matrix[0], "tp")
    flat_ids = selected_specialists.reshape(-1)
    one_hot = (flat_ids[:, None] == jnp.arange(experts, dtype=jnp.int32)[None, :]).astype(jnp.int32)
    slot_rank = jnp.sum((jnp.cumsum(one_hot, axis=0) - 1) * one_hot, axis=1)
    position = flat_ids * capacity + slot_rank
    placing = (position[:, None] == jnp.arange(slots, dtype=jnp.int32)[None, :]).reshape(
        tok_rows, top_count, slots
    )
    outgoing = jnp.einsum(
        "te,td->ed", jnp.sum(placing.astype(BF16), axis=1), normed, preferred_element_type=F32
    ).astype(BF16)
    weight = jnp.sum(jnp.where(placing, selection_mixing_factors[:, :, None], 0.0), axis=1)
    received = lax.all_to_all(
        outgoing.reshape(experts, capacity, model_width),
        "ep",
        split_axis=0,
        concat_axis=0,
        tiled=True,
    ).reshape(slots, model_width)

    omap, oloc, pay = run_local_mixer(
        query_vectors,
        attend_lookup_vectors,
        attend_content_vectors,
        forget_speed_dependent,
        amend_speed_dependent,
        feature_forget_baseline,
        amend_speed_baseline,
        sudden_forget_extra,
    )
    states = run_fold_states(pay)
    mixed_rows = run_finish_mixer(
        omap, oloc, states, result_switch_preactivation, group_scaling_factor
    )

    hidden = jnp.concatenate(
        [swiglu(received, gates[r], ups[r]) for r in range(tp_size)], axis=1
    )
    expert_rows = dot(hidden, downs.reshape(hidden.shape[1], model_width)).astype(BF16)
    expert_out = lax.all_to_all(
        expert_rows.reshape(experts, capacity, model_width),
        "ep",
        split_axis=0,
        concat_axis=0,
        tiled=True,
    ).reshape(slots, model_width)
    high = weight.astype(BF16)
    low = (weight - high.astype(F32)).astype(BF16)
    routed = dot(high, expert_out) + dot(low, expert_out)

    shared_hidden = swiglu(
        lax.all_gather(normed, "tp", axis=0, tiled=True),
        common_switch_matrix,
        common_raising_matrix,
    )
    shared_sum = lax.psum_scatter(
        dot(shared_hidden, common_lowering_matrix).astype(BF16),
        "tp",
        scatter_dimension=0,
        tiled=True,
    )
    attend = lax.psum_scatter(
        dot(mixed_rows, result_mapping_matrix).astype(BF16),
        "tp",
        scatter_dimension=0,
        tiled=True,
    )
    return (attend, (routed + shared_sum.astype(F32)).astype(BF16))


def solution(mesh):
    rows = P(("grp", "ep"), "tp")
    tokens = P(("grp", "ep", "tp"), None)
    placed = (
        (rows,) * 6
        + (P("tp"), P("tp"), rows, P("tp"), P("tp", None), tokens, P(), tokens, tokens)
        + (P("ep", None, "tp"), P("ep", None, "tp"), P("ep", "tp", None))
        + (P(None, "tp"), P(None, "tp"), P("tp", None))
    )
    return jax.shard_map(
        on_device, mesh=mesh, in_specs=placed, out_specs=(tokens, tokens), check_vma=False
    )
```

time: 951 us -> 423 us (0.44)
  other arithmetic: 366 us -> 4.4 us
  Pallas kernels: 0 us -> 123 us
  matrix products: 142 us -> 39 us
  waiting for transfers between devices: 278 us -> 183 us
  local copies, waits for them, and re-layouts: 108 us -> 19.2 us
    another operation x26 -> x2, other arithmetic: 329 us -> 0.63 us  [the longest x16 320 us: block_form(): jax.scipy.linalg.solve_triangular(identity[None] - erase_erase, solve_rhs...]
    pallas_call x0 -> x3, Pallas kernels: none -> 123 us  [the longest x1 90.7 us: run_fold_states(): pl.pallas_call(fold_states, in_specs=[vmem], out_specs=vmem, out_shape=ja...]
    dot_general x110 -> x15, matrix products: 130 us -> 39 us  [the longest x14 37.3 us: dot(): return jnp.dot(a, b, preferred_element_type=F32)]
    all_to_all x1, waiting for transfers between devices: 59.5 us -> 0.01 us  [on_device(): lax.all_to_all(expert_rows.reshape(experts, capacity, model_width), 'ep',...]
    dynamic_slice x81 -> x0, local copies, waits for them, and re-layouts: 41.2 us -> none  [the longest x64 33.5 us: step(): part[k].astype(own.dtype)]
    all_gather x3, waiting for transfers between devices: 104 us -> 66.1 us  [the longest x1 46.6 us: on_device(): downs = lax.all_gather(dispatched_lowering_matrix[0], 'tp')]
    mul x10 -> x0, other arithmetic: 23.9 us -> none  [the longest x8 18.1 us: block_form(): erase_span * tail_decay]
    all_gather x1, waiting for transfers between devices: 0.01 us -> 16.1 us  [on_device(): lax.all_gather(normed, 'tp', axis=0, tiled=True)]
  transfers between devices with their start and end apart: 8 -> 8, of which waited for: 5 -> 5; matrix products, arithmetic and copies ran while one was open for 62% -> 13% of each run, Pallas kernels for 0% -> 29%
where the time goes in v1:
time: 423 us; the launch traced here: 422 us
  waiting for transfers between devices  183 us (43%)
  Pallas kernels  123 us (29%)
  starting transfers between devices  39.8 us (9%)
  matrix products  39 us (9%)
  local copies, waits for them, and re-layouts  19.2 us (5%)
  between operations  14.5 us (3%)
  other arithmetic  4.4 us (1%)
    pallas_call x1, Pallas kernels, run_fold_states(): pl.pallas_call(fold_states, in_specs=[vmem], out_specs=vmem, out_shape=ja...  90.7 us
    all_to_all x1, waiting for transfers between devices, on_device(): lax.all_to_all(outgoing.reshape(experts, capacity, model_width), 'ep', sp...  74.4 us
    all_gather x1, waiting for transfers between devices, on_device(): downs = lax.all_gather(dispatched_lowering_matrix[0], 'tp')  46.6 us
    dot_general x14, matrix products, dot(): return jnp.dot(a, b, preferred_element_type=F32)  37.3 us
    pallas_call x1, Pallas kernels, run_local_mixer(): pl.pallas_call(local_mixer, grid=(width // lanes,), in_specs=[tall] * 5 +...  29 us
    all_to_all x1, starting transfers between devices, on_device(): lax.all_to_all(outgoing.reshape(experts, capacity, model_width), 'ep', sp...  25.6 us
    reduce_scatter x1, waiting for transfers between devices, on_device(): lax.psum_scatter(dot(mixed_rows, result_mapping_matrix).astype(BF16), 'tp...  24.2 us
    all_gather x1, waiting for transfers between devices, on_device(): ups = lax.all_gather(dispatched_raising_matrix[0], 'tp')  19.5 us
  transfers between devices with their start and end apart: 8, of which 5 were waited for; matrix products, arithmetic and copies ran while one was open for 13% of the time, Pallas kernels for 29%

profile of v1, /device:TPU:33, one launch (start us, length us, event | category | flops | bytes accessed | tf_op | source)
XLA Modules:
  0.0 422.4 jit_solution(887837065513263122)
XLA Ops:
  8.6 2.0 fusion.9
  16.5 3.6 reshape.79
  20.0 25.6 %all-to-all-start = ((bf16[32,12,2048]{2,1,0:T(8,128)(2,1)}), bf16[32,12,2048]{2,1,0:T(8,128)(2,1)}, u32[]{:S(2)}, u32[]{:S(2)}) async-start(bf16[32,12,2048]{2,1,0:T(8,128)(2,1)} %reshape.79), calls=%async_computation.1 | async-start | bytes 4194304 | tf_op jit(solution)/shard_map/all_to_all | solution.py:446
  46.0 16.1 %all-gather.11.cloned.1.call-done = bf16[512,2048]{1,0:T(8,128)(2,1)} async-done(((bf16[128,2048]{1,0:T(8,128)(2,1)}), bf16[512,2048]{1,0:T(8,128)(2,1)}) %all-gather.11.cloned.1.call-update) | async-done | bytes 2097168 | tf_op jit(solution)/shard_map/all_gather | solution.py:485
  62.2 2.3 fusion.37
  64.5 5.5 %convolution_convert_fusion = bf16[512,2048]{1,0:T(8,128)(2,1)} fusion(bf16[128,2048]{1,0:T(8,128)(2,1)} %param.41, bf16[512,2048]{1,0:T(8,128)(2,1)} %all-gather.11.cloned.1.call-done, bf16[2048,128]{1,0:T(8,128)(2,1)} %param.40, f32[512,128]{1,0:T(8,128)S(1)} %fusion.37), kind=kOutput, calls=%fused_computation | convolution fusion | flops 538312704 | bytes 5505024 | tf_op jit(solution)/shard_map/dot_general | solution.py:17
  70.0 74.4 %all-to-all-done = bf16[32,12,2048]{2,1,0:T(8,128)(2,1)} async-done(((bf16[32,12,2048]{2,1,0:T(8,128)(2,1)}), bf16[32,12,2048]{2,1,0:T(8,128)(2,1)}, u32[]{:S(2)}, u32[]{:S(2)}) %all-to-all-start) | async-done | bytes 1572896 | tf_op jit(solution)/shard_map/all_to_all | solution.py:446
  144.3 3.7 reshape.80
  148.0 3.3 fusion.13
  153.3 2.0 fusion.11
  155.3 19.5 %all-gather.7.cloned.1.call-done = bf16[4,2048,256]{2,1,0:T(8,128)(2,1)} async-done(((bf16[1,2048,256]{2,1,0:T(8,128)(2,1)}), bf16[4,2048,256]{2,1,0:T(8,128)(2,1)}) %all-gather.7.cloned.1.call-update) | async-done | bytes 4194320 | tf_op jit(solution)/shard_map/all_gather | solution.py:433
  174.8 2.7 fusion.2
  177.5 2.8 fusion.3
  184.6 46.6 %all-gather.9.cloned.1.call-done = bf16[4,256,2048]{2,1,0:T(8,128)(2,1)} async-done(((bf16[1,256,2048]{2,1,0:T(8,128)(2,1)}), bf16[4,256,2048]{2,1,0:T(8,128)(2,1)}) %all-gather.9.cloned.1.call-update) | async-done | bytes 4194320 | tf_op jit(solution)/shard_map/all_gather | solution.py:434
  231.2 5.3 %convolution_convert_fusion.2 = bf16[384,2048]{1,0:T(8,128)(2,1)} fusion(bf16[1024,2048]{1,0:T(8,128)(2,1)} %bitcast.66, bf16[384,256]{0,1:T(8,128)(2,1)} %fusion.5, bf16[384,256]{0,1:T(8,128)(2,1)S(1)} %fusion.4, bf16[384,256]{0,1:T(8,128)(2,1)S(1)} %copy-done.18, bf16[384,256]{0,1:T(8,128)(2,1)S(1)} %fusion.2), kind=kOutput, calls=%fused_computation.2 | convolution fusion | flops 1614544896 | bytes 6553600 | tf_op jit(solution)/shard_map/dot_general | solution.py:17
  236.5 3.6 reshape.82
  240.1 13.4 %all-to-all-start.1 = ((bf16[32,12,2048]{2,1,0:T(8,128)(2,1)}), bf16[32,12,2048]{2,1,0:T(8,128)(2,1)}, u32[]{:S(2)}, u32[]{:S(2)}) async-start(bf16[32,12,2048]{2,1,0:T(8,128)(2,1)} %reshape.82), calls=%async_computation.2 | async-start | bytes 4194304 | tf_op jit(solution)/shard_map/all_to_all | solution.py:473
  257.0 29.0 %local_mixer.1 = (bf16[512,512]{1,0:T(8,128)(2,1)S(1)}, f32[512,512]{1,0:T(8,128)S(1)}, bf16[32,48,128]{2,1,0:T(8,128)(2,1)S(1)}) custom-call(bf16[512,512]{1,0:T(8,128)(2,1)S(1)} %copy-done.1, bf16[512,512]{1,0:T(8,128)(2,1)S(1)} %copy-done.2, bf16[512,512]{1,0:T(8,128)(2,1)S(1)} %copy-done.3, bf16[512,512]{1,0:T(8,128)(2,1)S(1)} %copy-done.4, ...), custom_call_target="tpu_custom_call" | custom-call | flops 10000000000 | bytes 6000000 | tf_op jit(solution)/shard_map/local_mixer/pallas_call | solution.py:181
  286.0 90.7 %fold_states.1.state_ref = f32[32,8,128]{2,1,0:T(8,128)S(1)} custom-call(bf16[32,48,128]{2,1,0:T(8,128)(2,1)S(1)} %get-tuple-element.7.pay_ref), custom_call_target="tpu_custom_call" | custom-call | flops 20000000000 | bytes 3000000 | tf_op jit(solution)/shard_map/fold_states/pallas_call | solution.py:318
  376.7 2.9 finish_mixer.1
  379.6 2.6 convolution_convert_fusion.1
  383.1 3.7 reshape.83
  388.6 2.8 fusion.1
  391.4 24.2 %reduce-scatter.3.cloned.1.call-done = bf16[128,2048]{1,0:T(8,128)(2,1)} async-done(((bf16[512,2048]{1,0:T(8,128)(2,1)}), bf16[128,2048]{1,0:T(8,128)(2,1)}) %reduce-scatter.3.cloned.1.call-update) | async-done | bytes 524304 | tf_op jit(solution)/shard_map/reduce_scatter | solution.py:495
  (76 shorter events, 19.8 us)
Async XLA Ops:
  7.2 372.5 %copy-start = (bf16[512,2048]{1,0:T(8,128)(2,1)S(1)}, bf16[512,2048]{1,0:T(8,128)(2,1)}, u32[]{:S(2)}) copy-start(bf16[512,2048]{1,0:T(8,128)(2,1)} %param.31) | copy-start | bytes 6291460
  7.2 55.0 %all-gather.11.cloned.1.call-start = ((), (), s32[]{:S(2)}) async-start(), calls=%async_computation.8 | async-start | bytes 2621440 | tf_op jit(solution)/shard_map/all_gather | solution.py:485
  10.7 2.3 copy-start.15
  10.7 4.0 copy-start.10
  10.7 137.3 %all-gather.5.cloned.1.call-start = ((), (), s32[]{:S(2)}) async-start(), calls=%async_computation.5 | async-start | bytes 5242880 | tf_op jit(solution)/shard_map/all_gather | solution.py:432
  11.5 163.3 %all-gather.7.cloned.1.call-start = ((), (), s32[]{:S(2)}) async-start(), calls=%async_computation.6 | async-start | bytes 5242880 | tf_op jit(solution)/shard_map/all_gather | solution.py:433
  12.3 218.9 %all-gather.9.cloned.1.call-start = ((), (), s32[]{:S(2)}) async-start(), calls=%async_computation.7 | async-start | bytes 5242880 | tf_op jit(solution)/shard_map/all_gather | solution.py:434
  20.0 25.9 %copy-start.14 = (f32[512,8]{0,1:T(8,128)S(1)}, f32[512,8]{0,1:T(8,128)}, u32[]{:S(2)}) copy-start(f32[512,8]{0,1:T(8,128)} %param.29) | copy-start | bytes 49156
  20.0 42.1 %copy-start.13 = (bf16[2048,128]{1,0:T(8,128)(2,1)S(1)}, bf16[2048,128]{1,0:T(8,128)(2,1)}, u32[]{:S(2)}) copy-start(bf16[2048,128]{1,0:T(8,128)(2,1)} %param.39) | copy-start | bytes 1572868
  20.0 124.3 %all-to-all-start = ((bf16[32,12,2048]{2,1,0:T(8,128)(2,1)}), bf16[32,12,2048]{2,1,0:T(8,128)(2,1)}, u32[]{:S(2)}, u32[]{:S(2)}) async-start(bf16[32,12,2048]{2,1,0:T(8,128)(2,1)} %reshape.79), calls=%async_computation.1 | async-start | bytes 4194304 | tf_op jit(solution)/shard_map/all_to_all | solution.py:446
  45.6 343.0 %reduce-scatter.5.cloned.1.call-start = ((), (), s32[]{:S(2)}) async-start(), calls=%async_computation.9 | async-start | bytes 2621440 | tf_op jit(solution)/shard_map/reduce_scatter | solution.py:489
  148.0 3.3 copy-start.11
  174.8 2.7 copy-start.12
  177.5 2.8 copy-start.17
  183.1 48.1 %copy-start.18 = (bf16[384,256]{0,1:T(8,128)(2,1)S(1)}, bf16[384,256]{0,1:T(8,128)(2,1)}, u32[]{:S(2)}) copy-start(bf16[384,256]{0,1:T(8,128)(2,1)} %fusion.3) | copy-start | bytes 589828
  240.1 13.7 %copy-start.1 = (bf16[512,512]{1,0:T(8,128)(2,1)S(1)}, bf16[512,512]{1,0:T(8,128)(2,1)}, u32[]{:S(2)}) copy-start(bf16[512,512]{1,0:T(8,128)(2,1)} %q_ref.1) | copy-start | bytes 1572868
  240.1 13.7 %copy-start.2 = (bf16[512,512]{1,0:T(8,128)(2,1)S(1)}, bf16[512,512]{1,0:T(8,128)(2,1)}, u32[]{:S(2)}) copy-start(bf16[512,512]{1,0:T(8,128)(2,1)} %k_ref.1) | copy-start | bytes 1572868
  240.1 13.7 %copy-start.7 = (f32[512]{0:T(512)S(1)}, f32[512]{0:T(512)}, u32[]{:S(2)}) copy-start(f32[512]{0:T(512)} %param.27) | copy-start | bytes 6148
  240.1 13.8 %copy-start.8 = (f32[512]{0:T(512)S(1)}, f32[512]{0:T(512)}, u32[]{:S(2)}) copy-start(f32[512]{0:T(512)} %param.28) | copy-start | bytes 6148
  240.1 143.0 %all-to-all-start.1 = ((bf16[32,12,2048]{2,1,0:T(8,128)(2,1)}), bf16[32,12,2048]{2,1,0:T(8,128)(2,1)}, u32[]{:S(2)}, u32[]{:S(2)}) async-start(bf16[32,12,2048]{2,1,0:T(8,128)(2,1)} %reshape.82), calls=%async_computation.2 | async-start | bytes 4194304 | tf_op jit(solution)/shard_map/all_to_all | solution.py:473
  253.5 162.0 %reduce-scatter.3.cloned.1.call-start = ((), (), s32[]{:S(2)}) async-start(), calls=%async_computation.4 | async-start | bytes 2621440 | tf_op jit(solution)/shard_map/reduce_scatter | solution.py:495
  253.9 1.1 copy-start.3
  286.0 90.7 %copy-start.6 = (bf16[512,512]{1,0:T(8,128)(2,1)S(1)}, bf16[512,512]{1,0:T(8,128)(2,1)}, u32[]{:S(2)}) copy-start(bf16[512,512]{1,0:T(8,128)(2,1)} %gate_ref.1) | copy-start | bytes 1572868
  286.0 90.7 %copy-start.9 = (f32[512]{0:T(512)S(1)}, f32[512]{0:T(512)}, u32[]{:S(2)}) copy-start(f32[512]{0:T(512)} %param.30) | copy-start | bytes 6148
  (3 other events, 2.8 us)
Sparse Core Ops, SparseCore 0:
  10.9 51.2 all-gather.10
  64.0 54.3 all-gather.4
  120.2 54.6 all-gather.6
  176.5 54.6 all-gather.8
  233.6 36.2 reduce-scatter.4
  382.5 33.0 reduce-scatter.2

commit v2 on v1

v2 whole, which is shorter than its diff:
```python
import functools

import jax
import jax.numpy as jnp
from jax import lax
from jax.experimental import pallas as pl
from jax.experimental.pallas import tpu as pltpu
from jax.sharding import PartitionSpec as P

F32 = jnp.float32
BF16 = jnp.bfloat16
SPAN = 64
MESH = pl.DeviceIdType.MESH


def dot(a, b):
    return jnp.dot(a, b, preferred_element_type=F32)


def dot_nt(a, b):
    return lax.dot_general(a, b, (((1,), (1,)), ((), ())), preferred_element_type=F32)


def dot_tn(a, b):
    return lax.dot_general(a, b, (((0,), (0,)), ((), ())), preferred_element_type=F32)


def split(x, parts):
    out = []
    for _ in range(parts - 1):
        out.append(x.astype(BF16))
        x = x - out[-1].astype(F32)
    out.append(x.astype(BF16))
    return out


def iota(shape, dim):
    return lax.broadcasted_iota(jnp.int32, shape, dim)


def local_mixer(
    pair, q_ref, k_ref, v_ref, f_ref, a_ref, fb_ref, ab_ref, x_ref, omap_ref, oloc_ref, pay_ref
):
    rows = q_ref.shape[0]
    groups = x_ref.shape[0]
    half = q_ref.shape[1] // groups
    lanes = 2 * half
    spans = rows // SPAN
    here = pl.ds(pl.multiple_of(pair * lanes, lanes), lanes)
    low = iota((SPAN, lanes), 1) < half
    col = jnp.where(low, iota((SPAN, lanes), 1), iota((SPAN, lanes), 1) - half)
    row = iota((SPAN, lanes), 0)
    strict = row > col
    inclusive = row >= col
    tri = (iota((SPAN, SPAN), 0) >= iota((SPAN, SPAN), 1)).astype(BF16)
    tri3 = jnp.concatenate([tri] * 3, axis=1)
    same = ((iota((lanes, lanes), 0) < half) == (iota((lanes, lanes), 1) < half)).astype(BF16)
    same2 = jnp.concatenate([same] * 2, axis=0)
    spread = (
        iota((groups, lanes), 0) == 2 * pair + (iota((groups, lanes), 1) >= half).astype(jnp.int32)
    ).astype(F32)
    spread3 = jnp.concatenate([spread] * 3, axis=0).astype(BF16)
    below = iota((lanes, lanes), 0) < half
    left = iota((lanes, lanes), 1) < half

    def stack(x):
        return jnp.concatenate([jnp.where(low, x, 0.0), jnp.where(low, 0.0, x)], axis=0).astype(
            BF16
        )

    fb = fb_ref[:, here]
    ab = ab_ref[:, here]
    parts = [part.astype(F32) for part in split(x_ref[...], 3)]
    extra = dot_tn(jnp.concatenate(parts, axis=0).astype(BF16), spread3)

    spans_in = []
    for c in range(spans):
        at = slice(c * SPAN, (c + 1) * SPAN)
        decay = -jnp.exp(fb + f_ref[at, here].astype(F32)) + extra[at, :]
        rate = jax.nn.sigmoid(ab + a_ref[at, here].astype(F32))
        key = k_ref[at, here].astype(F32)
        sq = dot(jnp.concatenate(split(key * key, 2), axis=1), same2)
        unit = key * lax.rsqrt(sq + 1e-06)
        cum = dot(tri3, jnp.concatenate(split(decay, 3), axis=0))
        mid = cum[SPAN // 2 : SPAN // 2 + 1, :]
        last = cum[SPAN - 1 : SPAN, :]
        left_erase = -unit * jnp.exp(cum - decay - mid)
        left_read = q_ref[at, here].astype(F32) * jnp.exp(cum - mid)
        right = jnp.exp(mid - cum) * rate
        right_erase = unit * right
        right_write = key * right
        grow = jnp.exp(mid)
        tail = jnp.exp(last - mid)
        lefts = jnp.concatenate([left_erase, left_read], axis=0).astype(BF16)
        rights = jnp.concatenate([stack(right_erase), stack(right_write)], axis=0)
        pairs = dot_nt(lefts, rights)
        a_mat = jnp.where(strict, pairs[:SPAN, :lanes], 0.0)
        erase_write = jnp.where(strict, pairs[:SPAN, lanes:], 0.0)
        read_erase = jnp.where(inclusive, pairs[SPAN:, :lanes], 0.0)
        read_write = jnp.where(inclusive, pairs[SPAN:, lanes:], 0.0)
        value = v_ref[at, here].astype(F32)
        writes = dot(
            jnp.concatenate([erase_write, read_write], axis=0).astype(BF16), stack(value)
        )
        ends = jnp.concatenate([right_erase * tail, right_write * tail], axis=0).astype(BF16)
        spans_in.append(
            dict(
                a=a_mat,
                first=stack(left_erase * grow),
                read=left_read * grow,
                re=read_erase.astype(BF16),
                ew=stack(writes[:SPAN]),
                rw=writes[SPAN:],
                ends=ends,
                value=v_ref[at, here],
                last=jnp.exp(last),
            )
        )

    eye = (row == col).astype(F32)
    block = 1
    inverse = None
    while block < SPAN:
        in_block = (row // (2 * block) == col // (2 * block)) & (
            (row // block) % 2 == 1
        ) & ((col // block) % 2 == 0)
        steps = [jnp.where(in_block, s["a"], 0.0) for s in spans_in]
        if inverse is None:
            inverse = [eye + step for step in steps]
        else:
            inner = [
                dot(step.astype(BF16), stack(x)) for step, x in zip(steps, inverse)
            ]
            inverse = [x + dot(x.astype(BF16), stack(y)) for x, y in zip(inverse, inner)]
        block *= 2

    state = jnp.concatenate([eye, jnp.zeros_like(eye)], axis=0)
    for c, s in enumerate(spans_in):
        at = slice(c * SPAN, (c + 1) * SPAN)
        solved = dot(inverse[c].astype(BF16), jnp.concatenate([s["first"], s["ew"]], axis=1))
        w, y = (solved[:, :lanes], solved[:, lanes:])
        seen = dot(s["re"], jnp.concatenate([stack(w), stack(y)], axis=1))
        read = s["read"] + seen[:, :lanes]
        added = s["rw"] + seen[:, lanes:]
        value = s["value"]
        erased = dot_tn(w.astype(BF16), s["ends"][:SPAN])
        erased = jnp.where(below == left, erased, 0.0).astype(BF16)
        offset = dot_tn(jnp.concatenate([y.astype(BF16), value], axis=0), s["ends"])
        offset = jnp.where(low, offset[:half], offset[half:])
        both = jnp.concatenate([stack(state[:SPAN]), stack(state[SPAN:])], axis=0)
        reads = dot_nt(read.astype(BF16), both)
        omap_ref[at, here] = reads[:, :lanes].astype(BF16)
        oloc_ref[at, here] = added + reads[:, lanes:]
        state = (
            state * s["last"]
            + dot(state.astype(BF16), erased)
            + jnp.concatenate([jnp.zeros_like(offset), offset], axis=0)
        )
    jump, offset = (state[:SPAN], state[SPAN:])
    quarter = SPAN // 4
    eighth = SPAN // 8
    half_low = low[: SPAN // 2]
    jump_turned = pltpu.roll(jump, half, 1)
    offset_turned = pltpu.roll(offset, half, 1)
    empty = jnp.zeros((eighth, lanes), F32)
    for h in range(2):
        top = (jump, jump_turned)[h][: SPAN // 2]
        bottom = (jump_turned, jump)[h][SPAN // 2 :]
        packed = jnp.where(half_low, top, bottom)
        for j in range(4):
            top = (offset, offset_turned)[h][j * quarter : j * quarter + eighth]
            bottom = (offset_turned, offset)[h][j * quarter + eighth : (j + 1) * quarter]
            piece = jnp.where(low[:eighth], top, bottom)
            pay_ref[8 * pair + 4 * h + j] = jnp.concatenate([packed, piece, empty], axis=0).astype(
                BF16
            )


def fold_step(state, arrived):
    lanes = state.shape[1]
    half = lanes // 2
    low = iota((lanes // 4, lanes), 1) < half
    block = arrived.astype(F32)
    jump, offset = (block[: lanes // 4], block[lanes // 4 : lanes // 4 + 8])
    turned = pltpu.roll(jump, half, 1)
    spread = jnp.concatenate(
        [
            jnp.where(low, jump, 0.0),
            jnp.where(low, turned, 0.0),
            jnp.where(low, 0.0, turned),
            jnp.where(low, 0.0, jump),
        ],
        axis=0,
    ).astype(BF16)
    parts = [part.astype(F32) for part in split(state, 2)]
    moved = dot(jnp.concatenate(parts, axis=0).astype(BF16), spread)
    return moved[:8] + moved[8:] + offset


def finish_mixer(pair, omap_ref, oloc_ref, state_ref, gate_ref, gain_ref, out_ref):
    lanes = state_ref.shape[2]
    half = lanes // 2
    here = pl.ds(pl.multiple_of(pair * lanes, lanes), lanes)
    low = iota((8, lanes), 1) < half
    zero = jnp.zeros((8, lanes), F32)
    tiles = []
    for h in range(2):
        for j in range(4):
            block = state_ref[8 * pair + 4 * h + j]
            turned = pltpu.roll(block, half, 1)
            if h == 0:
                tiles += [jnp.where(low, block, zero), jnp.where(low, turned, zero)]
            else:
                tiles += [jnp.where(low, zero, turned), jnp.where(low, zero, block)]
    state = jnp.concatenate(tiles, axis=0).astype(BF16)
    same = jnp.where(
        (iota((lanes, lanes), 0) < half) == (iota((lanes, lanes), 1) < half), 1.0 / half, 0.0
    ).astype(BF16)
    same2 = jnp.concatenate([same] * 2, axis=0)
    head_out = oloc_ref[:, here] + dot_nt(omap_ref[:, here], state)
    mean = dot(jnp.concatenate(split(head_out, 2), axis=1), same2)
    centered = head_out - mean
    var = dot(jnp.concatenate(split(centered * centered, 2), axis=1), same2)
    normed = centered * lax.rsqrt(var + 0.00064) * gain_ref[:, here]
    out_ref[:, here] = (normed * jax.nn.sigmoid(gate_ref[:, here].astype(F32))).astype(BF16)


def slot_hits(ids, experts, capacity):
    tokens = ids.shape[1]
    ids = ids.astype(F32)
    expert = iota((experts, tokens), 0).astype(F32)
    hot = [(expert == ids[j : j + 1]).astype(F32) for j in range(2)]
    earlier = (iota((tokens, tokens), 0) < iota((tokens, tokens), 1)).astype(F32).astype(BF16)
    before = dot((hot[0] + hot[1]).astype(BF16), earlier)
    place = [
        ids[j : j + 1] * capacity + jnp.sum(hot[j] * before, axis=0, keepdims=True)
        for j in range(2)
    ]
    at = iota((16 * experts, tokens), 0)
    base = (capacity * (at // 16) + at % 4).astype(F32)
    quarter = (at // 4) % 4
    groups = [[base + 4 * g == place[j] for j in range(2)] for g in range(capacity // 4)]
    return groups, quarter


def everything(
    capacity,
    q_in,
    k_in,
    v_in,
    f_in,
    a_in,
    g_in,
    fb_ref,
    ab_ref,
    x_ref,
    gain_ref,
    wout_in,
    tok_ref,
    scale_ref,
    ids_ref,
    mix_ref,
    gate_in,
    up_in,
    down_in,
    cgate_in,
    cup_in,
    cdown_in,
    attend_ref,
    moe_ref,
    q_ref,
    k_ref,
    v_ref,
    f_ref,
    a_ref,
    g_ref,
    wout_ref,
    wg_ref,
    wu_ref,
    wd_ref,
    cgu_ref,
    cd_ref,
    omap_ref,
    oloc_ref,
    pay_ref,
    arrived,
    sent,
    states,
    mixed_ref,
    out_buf,
    in_buf,
    ret_buf,
    back_buf,
    xbuf,
    yacc,
    hbuf,
    normed_own,
    ngather,
    part_a,
    part_b,
    relay_a,
    relay_b,
    sums_a,
    sums_b,
    load_sem,
    own_sem,
    out_send,
    out_recv,
    pay_send,
    pay_recv,
    home_send,
    home_recv,
    ret_send,
    ret_recv,
    ring_send,
    ring_recv,
    rs_send,
    rs_recv,
):
    experts = out_buf.shape[0]
    tps = ngather.shape[0]
    tokens, width = tok_ref.shape
    quarter_width = width // 4
    groups = capacity // 4
    pairs = omap_ref.shape[1] // sent.shape[2]
    ep = lax.axis_index("ep")
    tp = lax.axis_index("tp")
    right, left, across = (lax.rem(tp + 1, tps), lax.rem(tp + 3, tps), lax.rem(tp + 2, tps))

    barrier = pltpu.get_barrier_semaphore()

    def greet(d, carry):
        pl.semaphore_signal(
            barrier, inc=1, device_id={"ep": lax.rem(ep + d, experts)}, device_id_type=MESH
        )
        return carry

    lax.fori_loop(1, experts, greet, 0)
    for near in (right, left):
        pl.semaphore_signal(barrier, inc=1, device_id={"tp": near}, device_id_type=MESH)

    half_lanes = cgate_in.shape[1]
    hid = gate_in.shape[1]
    loads = [
        pltpu.make_async_copy(a, b, load_sem.at[i])
        for i, (a, b) in enumerate(
            [
                (q_in, q_ref),
                (k_in, k_ref),
                (v_in, v_ref),
                (f_in, f_ref),
                (a_in, a_ref),
                (g_in, g_ref),
                (wout_in, wout_ref),
                (gate_in, wg_ref.at[0]),
                (up_in, wu_ref.at[0]),
                (down_in, wd_ref.at[pl.ds(0, hid)]),
                (cgate_in, cgu_ref.at[:, pl.ds(0, half_lanes)]),
                (cup_in, cgu_ref.at[:, pl.ds(half_lanes, half_lanes)]),
                (cdown_in, cd_ref),
            ]
        )
    ]
    for load in loads:
        load.start()

    def remote(src, dst, send, recv, axis, to):
        return pltpu.make_async_remote_copy(
            src_ref=src,
            dst_ref=dst,
            send_sem=send,
            recv_sem=recv,
            device_id={axis: to},
            device_id_type=MESH,
        )

    floats = tok_ref[...].astype(F32)
    normed = (
        floats
        * lax.rsqrt(jnp.mean(floats * floats, -1, keepdims=True) + 1e-06)
        * scale_ref[...]
    ).astype(BF16)
    normed_own[...] = normed
    hits, quarter = slot_hits(ids_ref[...], experts, capacity)
    stacked = jnp.concatenate(
        [normed[:, c * quarter_width : (c + 1) * quarter_width] for c in range(4)], axis=0
    )
    for g in range(groups):
        either = hits[g][0] | hits[g][1]
        placing = jnp.concatenate(
            [(either & (quarter == c)).astype(F32).astype(BF16) for c in range(4)], axis=1
        )
        out_buf[:, :, g * quarter_width : (g + 1) * quarter_width] = (
            dot(placing, stacked).astype(BF16).reshape(experts, 16, quarter_width)
        )

    pl.semaphore_wait(barrier, experts - 1 + 2)

    def peer(d):
        return lax.rem(ep + d, experts)

    def outward(d):
        to = peer(d)
        return remote(out_buf.at[to], in_buf.at[ep], out_send.at[d], out_recv.at[ep], "ep", to)

    def inward(d):
        e = peer(d)
        return remote(out_buf.at[e], in_buf.at[e], out_send.at[d], out_recv.at[e], "ep", e)

    def spray(make):
        def go(i, carry):
            d = experts // 2 - i
            make(d).start()
            make(experts - d).start()
            return carry

        make(experts // 2).start()
        lax.fori_loop(1, experts // 2, go, 0)

    def drain(make, recv):
        def go(d, carry):
            if recv:
                make(d).wait_recv()
            else:
                make(d).wait_send()
            return carry

        lax.fori_loop(1, experts, go, 0)

    spray(outward)

    class Ring:
        def __init__(self, index, own, slot):
            n = own.shape[0]
            top, bottom = (pl.ds(0, n // 2), pl.ds(n // 2, n // 2))
            s = [ring_send.at[4 * index + i] for i in range(4)]
            r = [ring_recv.at[4 * index + i] for i in range(4)]
            self.near = [
                remote(own, slot(1, pl.ds(0, n)), s[0], r[0], "tp", right),
                remote(own, slot(2, pl.ds(0, n)), s[1], r[1], "tp", left),
            ]
            self.far = [
                remote(slot(1, top), slot(3, top), s[2], r[2], "tp", right),
                remote(slot(2, bottom), slot(3, bottom), s[3], r[3], "tp", left),
            ]

        def start(self):
            for copy in self.near:
                copy.start()

        def forward(self):
            for copy, onward in zip(self.near, self.far):
                copy.wait_recv()
                onward.start()

        def arrive(self):
            for copy in self.far:
                copy.wait_recv()

        def finish(self):
            for copy in self.near + self.far:
                copy.wait_send()

    gate_ring = Ring(0, gate_in, lambda s, rows: wg_ref.at[s, rows])
    up_ring = Ring(1, up_in, lambda s, rows: wu_ref.at[s, rows])
    down_ring = Ring(
        2, down_in, lambda s, rows: wd_ref.at[pl.ds(s * hid + rows.start, rows.size)]
    )
    normed_ring = Ring(3, normed_own, lambda s, rows: ngather.at[s, rows])
    weight_rings = (gate_ring, up_ring, down_ring)
    for ring in weight_rings:
        ring.start()

    own_out = pltpu.make_async_copy(out_buf.at[ep], in_buf.at[ep], own_sem.at[0])
    own_out.start()
    own_normed = pltpu.make_async_copy(normed_own, ngather.at[0], own_sem.at[1])
    own_normed.start()

    for load in loads[:5]:
        load.wait()

    def mix(pair, carry):
        local_mixer(
            pair,
            q_ref,
            k_ref,
            v_ref,
            f_ref,
            a_ref,
            fb_ref,
            ab_ref,
            x_ref,
            omap_ref,
            oloc_ref,
            pay_ref,
        )
        return carry

    lax.fori_loop(0, pairs, mix, 0)

    def pay_out(d):
        to = peer(d)
        return remote(pay_ref.at[to], arrived.at[ep], pay_send.at[d], pay_recv.at[ep], "ep", to)

    def pay_in(e):
        return remote(pay_ref.at[e], arrived.at[e], pay_send.at[0], pay_recv.at[e], "ep", e)

    spray(pay_out)
    own_pay = pltpu.make_async_copy(pay_ref.at[ep], arrived.at[ep], own_sem.at[2])
    own_pay.start()

    for ring in weight_rings:
        ring.forward()
    normed_ring.start()

    own_out.wait()
    drain(inward, True)
    block_rows = 4 * experts
    at_row = iota((block_rows, 16 * experts), 0)
    at_col = iota((block_rows, 16 * experts), 1)
    for c in range(4):
        pick = (at_col == 16 * (at_row // 4) + 4 * c + at_row % 4).astype(F32).astype(BF16)
        for g in range(groups):
            block = in_buf[:, :, g * quarter_width : (g + 1) * quarter_width].reshape(
                16 * experts, quarter_width
            )
            xbuf[
                g * block_rows : (g + 1) * block_rows,
                c * quarter_width : (c + 1) * quarter_width,
            ] = dot(pick, block).astype(BF16)

    for load in loads[7:10]:
        load.wait()

    def hidden(s):
        rows = xbuf[...]
        return (jax.nn.silu(dot(rows, wg_ref[s])) * dot(rows, wu_ref[s])).astype(BF16)

    for s in range(3):
        hbuf[:, s * hid : (s + 1) * hid] = hidden(s)
    yacc[...] = dot(hbuf[...], wd_ref[: 3 * hid])

    own_pay.wait()

    def homeward(e):
        return remote(sent.at[e], states.at[ep], home_send.at[e], home_recv.at[ep], "ep", e)

    def home(e):
        return remote(sent.at[e], states.at[e], home_send.at[e], home_recv.at[e], "ep", e)

    def step(e, state):
        sent[e] = state

        @pl.when(e != ep)
        def _():
            pay_in(e).wait_recv()

        @pl.when((e > 0) & (e - 1 != ep))
        def _():
            homeward(e - 1).start()

        return fold_step(state, arrived[e])

    lax.fori_loop(0, experts, step, jnp.zeros(sent.shape[1:], F32))

    @pl.when(ep != experts - 1)
    def _():
        homeward(experts - 1).start()

    own_state = pltpu.make_async_copy(sent.at[ep], states.at[ep], own_sem.at[3])
    own_state.start()

    for ring in weight_rings:
        ring.arrive()
    total = yacc[...] + dot(hidden(3), wd_ref[3 * hid :])
    yacc[...] = total
    at_row = iota((16 * experts, block_rows), 0)
    at_col = iota((16 * experts, block_rows), 1)
    put = jnp.concatenate(
        [
            (at_row == 16 * (at_col // 4) + 4 * c + at_col % 4).astype(F32).astype(BF16)
            for c in range(4)
        ],
        axis=1,
    )
    for g in range(groups):
        rows = yacc[g * block_rows : (g + 1) * block_rows, :].astype(BF16)
        rows = jnp.concatenate(
            [rows[:, c * quarter_width : (c + 1) * quarter_width] for c in range(4)], axis=0
        )
        ret_buf[:, :, g * quarter_width : (g + 1) * quarter_width] = (
            dot(put, rows).astype(BF16).reshape(experts, 16, quarter_width)
        )

    def ret_out(d):
        to = peer(d)
        return remote(ret_buf.at[to], back_buf.at[ep], ret_send.at[d], ret_recv.at[ep], "ep", to)

    def ret_in(d):
        e = peer(d)
        return remote(ret_buf.at[e], back_buf.at[e], ret_send.at[d], ret_recv.at[e], "ep", e)

    spray(ret_out)
    own_ret = pltpu.make_async_copy(ret_buf.at[ep], back_buf.at[ep], own_sem.at[4])
    own_ret.start()

    def homecoming(d, carry):
        home(peer(d)).wait_recv()
        return carry

    lax.fori_loop(1, experts, homecoming, 0)
    own_state.wait()
    for load in loads[5:7]:
        load.wait()

    def finish(pair, carry):
        finish_mixer(pair, omap_ref, oloc_ref, states, g_ref, gain_ref, mixed_ref)
        return carry

    lax.fori_loop(0, pairs, finish, 0)

    class Scatter:
        def __init__(self, index, part, relay, sums):
            n = part.shape[1]
            top, bottom = (pl.ds(0, n // 2), pl.ds(n // 2, n // 2))
            s = [rs_send.at[6 * index + i] for i in range(6)]
            r = [rs_recv.at[6 * index + i] for i in range(6)]
            self.part, self.sums = (part, sums)
            self.near = [
                remote(part.at[3, top], relay.at[0], s[0], r[0], "tp", right),
                remote(part.at[3, bottom], relay.at[1], s[1], r[1], "tp", left),
                remote(part.at[2], sums.at[1], s[2], r[2], "tp", right),
                remote(part.at[1], sums.at[2], s[3], r[3], "tp", left),
            ]
            self.far = [
                remote(relay.at[0], sums.at[3, top], s[4], r[4], "tp", right),
                remote(relay.at[1], sums.at[3, bottom], s[5], r[5], "tp", left),
            ]

        def start(self):
            for copy in self.near:
                copy.start()

        def forward(self):
            for copy, onward in zip(self.near[:2], self.far):
                copy.wait_recv()
                onward.start()

        def total(self):
            for copy in self.near[2:] + self.far:
                copy.wait_recv()
            out = self.part[0].astype(F32)
            for s in range(1, 4):
                out = out + self.sums[s].astype(F32)
            return out

        def finish(self):
            for copy in self.near + self.far:
                copy.wait_send()

    scatter_a = Scatter(0, part_a, relay_a, sums_a)
    scatter_b = Scatter(1, part_b, relay_b, sums_b)
    mixer_rows = part_a.shape[1]
    for s, owner in enumerate((tp, left, right, across)):
        mine = pl.ds(pl.multiple_of(owner * mixer_rows, mixer_rows), mixer_rows)
        part_a[s] = dot(mixed_ref[mine, :], wout_ref[...]).astype(BF16)
    scatter_a.start()

    normed_ring.forward()
    own_normed.wait()
    for load in loads[10:13]:
        load.wait()
    normed_ring.arrive()
    scatter_a.forward()
    both = dot(ngather[...].reshape(tps * tokens, width), cgu_ref[...])
    inner = (jax.nn.silu(both[:, :half_lanes]) * both[:, half_lanes:]).astype(BF16)
    for s in range(4):
        part_b[s] = dot(inner[s * tokens : (s + 1) * tokens], cd_ref[...]).astype(BF16)
    scatter_b.start()
    scatter_b.forward()
    attend_ref[...] = scatter_a.total().astype(BF16)
    moe_sum = scatter_b.total()
    yacc[:tokens, :] = moe_sum

    hits, quarter = slot_hits(ids_ref[...], experts, capacity)
    own_ret.wait()
    drain(ret_in, True)
    for c in range(4):
        block = yacc[:tokens, c * quarter_width : (c + 1) * quarter_width]
        for g in range(groups):
            weight = jnp.where(hits[g][0], mix_ref[0:1, :], 0.0) + jnp.where(
                hits[g][1], mix_ref[1:2, :], 0.0
            )
            weight = jnp.where(quarter == c, weight, 0.0)
            values = back_buf[:, :, g * quarter_width : (g + 1) * quarter_width].reshape(
                16 * experts, quarter_width
            )
            for part in split(weight, 2):
                block = block + dot_tn(part, values)
        moe_ref[:, c * quarter_width : (c + 1) * quarter_width] = block.astype(BF16)

    drain(outward, False)
    drain(pay_out, False)
    drain(ret_out, False)

    def homegoing(d, carry):
        homeward(peer(d)).wait_send()
        return carry

    lax.fori_loop(1, experts, homegoing, 0)
    for item in weight_rings + (normed_ring, scatter_a, scatter_b):
        item.finish()


def on_device(
    query_vectors,
    attend_lookup_vectors,
    attend_content_vectors,
    forget_speed_dependent,
    amend_speed_dependent,
    result_switch_preactivation,
    feature_forget_baseline,
    amend_speed_baseline,
    sudden_forget_extra,
    group_scaling_factor,
    result_mapping_matrix,
    specialist_tokens_activations,
    specialist_scaling_factor,
    selected_specialists,
    selection_mixing_factors,
    dispatched_switch_matrix,
    dispatched_raising_matrix,
    dispatched_lowering_matrix,
    common_switch_matrix,
    common_raising_matrix,
    common_lowering_matrix,
):
    tokens, top_count = selected_specialists.shape
    width = specialist_tokens_activations.shape[1]
    rows, mix_width = query_vectors.shape
    groups = sudden_forget_extra.shape[1]
    lanes = 2 * (mix_width // groups)
    experts = lax.axis_size("ep")
    tps = lax.axis_size("tp")
    capacity = 3 * tokens * top_count // (2 * experts)
    hid = dispatched_switch_matrix.shape[2]
    shared = common_switch_matrix.shape[1]
    slab = (experts, 16, capacity * width // 16)
    vmem = pl.BlockSpec(memory_space=pltpu.VMEM)
    hbm = pl.BlockSpec(memory_space=pl.ANY)
    V = pltpu.VMEM
    dma = pltpu.SemaphoreType.DMA
    mixer_rows = rows // tps
    return pl.pallas_call(
        functools.partial(everything, capacity),
        in_specs=[hbm] * 6 + [vmem] * 4 + [hbm] + [vmem] * 4 + [hbm] * 6,
        out_specs=(vmem, vmem),
        out_shape=(
            jax.ShapeDtypeStruct((mixer_rows, width), BF16),
            jax.ShapeDtypeStruct((tokens, width), BF16),
        ),
        scratch_shapes=[V((rows, mix_width), BF16)] * 6
        + [
            V((mix_width, width), BF16),
            V((tps, width, hid), BF16),
            V((tps, width, hid), BF16),
            V((tps * hid, width), BF16),
            V((width, 2 * shared), BF16),
            V((shared, width), BF16),
            V((rows, mix_width), BF16),
            V((rows, mix_width), F32),
            V((experts, 48, lanes), BF16),
            V((experts, 48, lanes), BF16),
            V((experts, 8, lanes), F32),
            V((experts, 8, lanes), F32),
            V((rows, mix_width), BF16),
        ]
        + [V(slab, BF16)] * 4
        + [
            V((experts * capacity, width), BF16),
            V((experts * capacity, width), F32),
            V((experts * capacity, 3 * hid), BF16),
            V((tokens, width), BF16),
            V((tps, tokens, width), BF16),
            V((tps, mixer_rows, width), BF16),
            V((tps, tokens, width), BF16),
            V((2, mixer_rows // 2, width), BF16),
            V((2, tokens // 2, width), BF16),
            V((tps, mixer_rows, width), BF16),
            V((tps, tokens, width), BF16),
            dma((13,)),
            dma((5,)),
        ]
        + [dma((experts,))] * 8
        + [dma((16,)), dma((16,)), dma((12,)), dma((12,))],
        compiler_params=pltpu.CompilerParams(
            collective_id=0, has_side_effects=True, vmem_limit_bytes=62 * 1024 * 1024
        ),
        name="everything",
    )(
        query_vectors,
        attend_lookup_vectors,
        attend_content_vectors,
        forget_speed_dependent,
        amend_speed_dependent,
        result_switch_preactivation,
        feature_forget_baseline.reshape(1, -1),
        amend_speed_baseline.reshape(1, -1),
        sudden_forget_extra.T,
        group_scaling_factor.reshape(1, -1),
        result_mapping_matrix,
        specialist_tokens_activations,
        specialist_scaling_factor.reshape(1, -1),
        selected_specialists.T,
        selection_mixing_factors.T,
        dispatched_switch_matrix[0],
        dispatched_raising_matrix[0],
        dispatched_lowering_matrix[0],
        common_switch_matrix,
        common_raising_matrix,
        common_lowering_matrix,
    )


def solution(mesh):
    rows = P(("grp", "ep"), "tp")
    tokens = P(("grp", "ep", "tp"), None)
    placed = (
        (rows,) * 6
        + (P("tp"), P("tp"), rows, P("tp"), P("tp", None), tokens, P(), tokens, tokens)
        + (P("ep", None, "tp"), P("ep", None, "tp"), P("ep", "tp", None))
        + (P(None, "tp"), P(None, "tp"), P("tp", None))
    )
    return jax.shard_map(
        on_device, mesh=mesh, in_specs=placed, out_specs=(tokens, tokens), check_vma=False
    )
```

time: 423 us -> 214 us (0.51)
  waiting for transfers between devices: 183 us -> 0 us
  Pallas kernels: 123 us -> 209 us
  starting transfers between devices: 39.8 us -> 0 us
  matrix products: 39 us -> 0 us
  local copies, waits for them, and re-layouts: 19.2 us -> 3.76 us
  between operations: 14.5 us -> 0.65 us
  other arithmetic: 4.4 us -> 0 us
    pallas_call x3 -> x1, Pallas kernels: 123 us -> 209 us  [on_device(): pl.pallas_call(functools.partial(everything, capacity), in_specs=[hbm] *...]
    all_gather x4 -> x0, waiting for transfers between devices: 82.3 us -> none  [the longest x1 46.6 us: on_device(): downs = lax.all_gather(dispatched_lowering_matrix[0], 'tp')]
    all_to_all x2 -> x0, waiting for transfers between devices: 74.4 us -> none  [the longest x1 74.4 us: on_device(): lax.all_to_all(outgoing.reshape(experts, capacity, model_width), 'ep', sp...]
    dot_general x15 -> x0, matrix products: 39 us -> none  [the longest x14 37.3 us: dot(): return jnp.dot(a, b, preferred_element_type=F32)]
    all_to_all x2 -> x0, starting transfers between devices: 39 us -> none  [the longest x1 25.6 us: on_device(): lax.all_to_all(outgoing.reshape(experts, capacity, model_width), 'ep', sp...]
    reduce_scatter x2 -> x0, waiting for transfers between devices: 24.2 us -> none  [the longest x1 24.2 us: on_device(): lax.psum_scatter(dot(mixed_rows, result_mapping_matrix).astype(BF16), 'tp...]
    reshape x4 -> x0, local copies, waits for them, and re-layouts: 14.5 us -> none  [the longest x1 3.65 us: on_device(): received = lax.all_to_all(outgoing.reshape(experts, capacity, model_width...]
  transfers between devices with their start and end apart: 8 -> 0, of which waited for: 5 -> 0; matrix products, arithmetic and copies ran while one was open for 13% -> 0% of each run, Pallas kernels for 29% -> 0%
where the time goes in v2:
time: 214 us
  Pallas kernels  209 us (98%)
  local copies, waits for them, and re-layouts  3.76 us (2%)
    pallas_call x1, Pallas kernels, on_device(): pl.pallas_call(functools.partial(everything, capacity), in_specs=[hbm] *...  209 us

profile of v2, /device:TPU:33, one launch (start us, length us, event | category | flops | bytes accessed | tf_op | source)
XLA Modules:
  0.0 213.7 jit_solution(13712652985593058104)
XLA Ops:
  0.6 209.3 %everything.1 = (bf16[128,2048]{1,0:T(8,128)(2,1)}, bf16[128,2048]{1,0:T(8,128)(2,1)}) custom-call(bf16[512,512]{1,0:T(8,128)(2,1)} %q_in.1, bf16[512,512]{1,0:T(8,128)(2,1)} %k_in.1, bf16[512,512]{1,0:T(8,128)(2,1)} %v_in.1, bf16[512,512]{1,0:T(8,128)(2,1)} %f_in.1, bf16[512,512]{1,0:T(8,128)(2,1)} %a_in.1, bf16[512,512]{1,0:T(8,128)(2,1)} %g_in.1, ...), custom_call_target="tpu_custom_call" | custom-call | tf_op jit(solution)/shard_map/everything/pallas_call | solution.py:754
  209.9 1.9 copy.25
  211.8 1.9 copy.26

commit v3 on v2

--- a/solution.py
+++ b/solution.py
@@ -157,31 +157,24 @@
             + jnp.concatenate([jnp.zeros_like(offset), offset], axis=0)
         )
     jump, offset = (state[:SPAN], state[SPAN:])
-    quarter = SPAN // 4
-    eighth = SPAN // 8
-    half_low = low[: SPAN // 2]
     jump_turned = pltpu.roll(jump, half, 1)
     offset_turned = pltpu.roll(offset, half, 1)
-    empty = jnp.zeros((eighth, lanes), F32)
+    near = low[: SPAN // 2]
     for h in range(2):
-        top = (jump, jump_turned)[h][: SPAN // 2]
-        bottom = (jump_turned, jump)[h][SPAN // 2 :]
-        packed = jnp.where(half_low, top, bottom)
-        for j in range(4):
-            top = (offset, offset_turned)[h][j * quarter : j * quarter + eighth]
-            bottom = (offset_turned, offset)[h][j * quarter + eighth : (j + 1) * quarter]
-            piece = jnp.where(low[:eighth], top, bottom)
-            pay_ref[8 * pair + 4 * h + j] = jnp.concatenate([packed, piece, empty], axis=0).astype(
-                BF16
-            )
+        packed = [
+            jnp.where(near, (x, turned)[h][: SPAN // 2], (turned, x)[h][SPAN // 2 :])
+            for x, turned in ((jump, jump_turned), (offset, offset_turned))
+        ]
+        pay_ref[2 * pair + h] = jnp.concatenate(packed, axis=0).astype(BF16)
 
 
 def fold_step(state, arrived):
     lanes = state.shape[1]
     half = lanes // 2
-    low = iota((lanes // 4, lanes), 1) < half
+    low = iota(state.shape, 1) < half
     block = arrived.astype(F32)
-    jump, offset = (block[: lanes // 4], block[lanes // 4 : lanes // 4 + 8])
+    rows = state.shape[0]
+    jump, offset = (block[:rows], block[rows:])
     turned = pltpu.roll(jump, half, 1)
     spread = jnp.concatenate(
         [
@@ -194,24 +187,22 @@
     ).astype(BF16)
     parts = [part.astype(F32) for part in split(state, 2)]
     moved = dot(jnp.concatenate(parts, axis=0).astype(BF16), spread)
-    return moved[:8] + moved[8:] + offset
+    return moved[:rows] + moved[rows:] + offset
 
 
 def finish_mixer(pair, omap_ref, oloc_ref, state_ref, gate_ref, gain_ref, out_ref):
     lanes = state_ref.shape[2]
     half = lanes // 2
     here = pl.ds(pl.multiple_of(pair * lanes, lanes), lanes)
-    low = iota((8, lanes), 1) < half
-    zero = jnp.zeros((8, lanes), F32)
+    low = iota(state_ref.shape[1:], 1) < half
     tiles = []
     for h in range(2):
-        for j in range(4):
-            block = state_ref[8 * pair + 4 * h + j]
-            turned = pltpu.roll(block, half, 1)
-            if h == 0:
-                tiles += [jnp.where(low, block, zero), jnp.where(low, turned, zero)]
-            else:
-                tiles += [jnp.where(low, zero, turned), jnp.where(low, zero, block)]
+        block = state_ref[2 * pair + h]
+        turned = pltpu.roll(block, half, 1)
+        if h == 0:
+            tiles += [jnp.where(low, block, 0.0), jnp.where(low, turned, 0.0)]
+        else:
+            tiles += [jnp.where(low, 0.0, turned), jnp.where(low, 0.0, block)]
     state = jnp.concatenate(tiles, axis=0).astype(BF16)
     same = jnp.where(
         (iota((lanes, lanes), 0) < half) == (iota((lanes, lanes), 1) < half), 1.0 / half, 0.0
@@ -326,6 +317,14 @@
     ep = lax.axis_index("ep")
     tp = lax.axis_index("tp")
     right, left, across = (lax.rem(tp + 1, tps), lax.rem(tp + 3, tps), lax.rem(tp + 2, tps))
+    paired = lax.axis_size("grp") % 2 == 0
+    grp = lax.axis_index("grp")
+    side = lax.rem(grp, 2)
+    partner = grp + 1 - 2 * side
+    heads = pay_ref.shape[0]
+    stride = experts // heads
+    my_head = ep // stride
+    folds = lax.rem(ep, stride) == 0
 
     barrier = pltpu.get_barrier_semaphore()
 
@@ -338,6 +337,8 @@
     lax.fori_loop(1, experts, greet, 0)
     for near in (right, left):
         pl.semaphore_signal(barrier, inc=1, device_id={"tp": near}, device_id_type=MESH)
+    if paired:
+        pl.semaphore_signal(barrier, inc=1, device_id={"grp": partner}, device_id_type=MESH)
 
     half_lanes = cgate_in.shape[1]
     hid = gate_in.shape[1]
@@ -394,7 +395,7 @@
             dot(placing, stacked).astype(BF16).reshape(experts, 16, quarter_width)
         )
 
-    pl.semaphore_wait(barrier, experts - 1 + 2)
+    pl.semaphore_wait(barrier, experts - 1 + 2 + int(paired))
 
     def peer(d):
         return lax.rem(ep + d, experts)
@@ -407,15 +408,16 @@
         e = peer(d)
         return remote(out_buf.at[e], in_buf.at[e], out_send.at[d], out_recv.at[e], "ep", e)
 
-    def spray(make):
+    def spray(make, first, last):
         def go(i, carry):
             d = experts // 2 - i
             make(d).start()
             make(experts - d).start()
             return carry
 
-        make(experts // 2).start()
-        lax.fori_loop(1, experts // 2, go, 0)
+        if first == 0:
+            make(experts // 2).start()
+        lax.fori_loop(max(first, 1), last, go, 0)
 
     def drain(make, recv):
         def go(d, carry):
@@ -427,31 +429,57 @@
 
         lax.fori_loop(1, experts, go, 0)
 
-    spray(outward)
+    spray(outward, 0, experts // 2)
 
     class Ring:
-        def __init__(self, index, own, slot):
+        def __init__(self, index, own, slot, pair_left, pair_right):
             n = own.shape[0]
-            top, bottom = (pl.ds(0, n // 2), pl.ds(n // 2, n // 2))
-            s = [ring_send.at[4 * index + i] for i in range(4)]
-            r = [ring_recv.at[4 * index + i] for i in range(4)]
-            self.near = [
-                remote(own, slot(1, pl.ds(0, n)), s[0], r[0], "tp", right),
-                remote(own, slot(2, pl.ds(0, n)), s[1], r[1], "tp", left),
-            ]
-            self.far = [
-                remote(slot(1, top), slot(3, top), s[2], r[2], "tp", right),
-                remote(slot(2, bottom), slot(3, bottom), s[3], r[3], "tp", left),
-            ]
+            mine = pl.ds(pl.multiple_of(side * (n // 2), n // 2), n // 2)
+            other = pl.ds(pl.multiple_of((1 - side) * (n // 2), n // 2), n // 2)
+            whole = pl.ds(0, n)
+            s = [ring_send.at[6 * index + i] for i in range(6)]
+            r = [ring_recv.at[6 * index + i] for i in range(6)]
+            self.near, self.far, self.pair, self.paired_in = ([], [], [], [])
+            for i, (to, half, rest, pair) in enumerate(
+                [
+                    (right, mine, other, paired and pair_left),
+                    (left, other, mine, paired and pair_right),
+                ]
+            ):
+                part = half if pair else whole
+                self.near.append(
+                    remote(own.at[part], slot(i + 1, part), s[i], r[i], "tp", to)
+                )
+                self.far.append(
+                    remote(slot(i + 1, half), slot(3, half), s[2 + i], r[2 + i], "tp", to)
+                )
+                self.pair.append(
+                    pair
+                    and (
+                        remote(
+                            slot(i + 1, half), slot(i + 1, half), s[4 + i], r[4 + i], "grp", partner
+                        ),
+                        remote(
+                            slot(i + 1, rest), slot(i + 1, rest), s[4 + i], r[4 + i], "grp", partner
+                        ),
+                    )
+                )
 
         def start(self):
             for copy in self.near:
                 copy.start()
 
         def forward(self):
-            for copy, onward in zip(self.near, self.far):
+            for copy, onward, pair in zip(self.near, self.far, self.pair):
                 copy.wait_recv()
                 onward.start()
+                if pair:
+                    pair[0].start()
+
+        def beside(self):
+            for pair in self.pair:
+                if pair:
+                    pair[1].wait_recv()
 
         def arrive(self):
             for copy in self.far:
@@ -460,14 +488,24 @@
         def finish(self):
             for copy in self.near + self.far:
                 copy.wait_send()
-
-    gate_ring = Ring(0, gate_in, lambda s, rows: wg_ref.at[s, rows])
-    up_ring = Ring(1, up_in, lambda s, rows: wu_ref.at[s, rows])
-    down_ring = Ring(
-        2, down_in, lambda s, rows: wd_ref.at[pl.ds(s * hid + rows.start, rows.size)]
-    )
-    normed_ring = Ring(3, normed_own, lambda s, rows: ngather.at[s, rows])
-    weight_rings = (gate_ring, up_ring, down_ring)
+            for pair in self.pair:
+                if pair:
+                    pair[0].wait_send()
+
+    def down_slot(base):
+        def slot(s, rows):
+            return wd_ref.at[pl.ds(pl.multiple_of(s * hid + base + rows.start, hid // 4), rows.size)]
+
+        return slot
+
+    gate_ring = Ring(0, gate_in, lambda s, rows: wg_ref.at[s, rows], True, True)
+    up_ring = Ring(1, up_in, lambda s, rows: wu_ref.at[s, rows], True, True)
+    down_rings = [
+        Ring(2, down_in.at[pl.ds(0, hid // 2)], down_slot(0), True, False),
+        Ring(3, down_in.at[pl.ds(hid // 2, hid // 2)], down_slot(hid // 2), False, True),
+    ]
+    normed_ring = Ring(4, normed_own, lambda s, rows: ngather.at[s, rows], False, False)
+    weight_rings = (gate_ring, up_ring, *down_rings)
     for ring in weight_rings:
         ring.start()
 
@@ -480,6 +518,10 @@
         load.wait()
 
     def mix(pair, carry):
+        @pl.when(pair == pairs // 2)
+        def _():
+            gate_ring.forward()
+
         local_mixer(
             pair,
             q_ref,
@@ -498,18 +540,26 @@
 
     lax.fori_loop(0, pairs, mix, 0)
 
-    def pay_out(d):
-        to = peer(d)
-        return remote(pay_ref.at[to], arrived.at[ep], pay_send.at[d], pay_recv.at[ep], "ep", to)
+    def pay_out(h):
+        return remote(
+            pay_ref.at[h], arrived.at[ep], pay_send.at[h], pay_recv.at[ep], "ep", stride * h
+        )
 
     def pay_in(e):
-        return remote(pay_ref.at[e], arrived.at[e], pay_send.at[0], pay_recv.at[e], "ep", e)
-
-    spray(pay_out)
-    own_pay = pltpu.make_async_copy(pay_ref.at[ep], arrived.at[ep], own_sem.at[2])
-    own_pay.start()
-
-    for ring in weight_rings:
+        return remote(pay_ref.at[0], arrived.at[e], pay_send.at[0], pay_recv.at[e], "ep", e)
+
+    def others(act):
+        for h in range(heads):
+            pl.when(ep != stride * h)(functools.partial(act, h))
+
+    others(lambda h: pay_out(h).start())
+    own_pay = pltpu.make_async_copy(pay_ref.at[my_head], arrived.at[ep], own_sem.at[2])
+
+    @pl.when(folds)
+    def _():
+        own_pay.start()
+
+    for ring in weight_rings[1:]:
         ring.forward()
     normed_ring.start()
 
@@ -536,39 +586,13 @@
         rows = xbuf[...]
         return (jax.nn.silu(dot(rows, wg_ref[s])) * dot(rows, wu_ref[s])).astype(BF16)
 
+    gate_ring.beside()
+    up_ring.beside()
     for s in range(3):
         hbuf[:, s * hid : (s + 1) * hid] = hidden(s)
+    for ring in down_rings:
+        ring.beside()
     yacc[...] = dot(hbuf[...], wd_ref[: 3 * hid])
-
-    own_pay.wait()
-
-    def homeward(e):
-        return remote(sent.at[e], states.at[ep], home_send.at[e], home_recv.at[ep], "ep", e)
-
-    def home(e):
-        return remote(sent.at[e], states.at[e], home_send.at[e], home_recv.at[e], "ep", e)
-
-    def step(e, state):
-        sent[e] = state
-
-        @pl.when(e != ep)
-        def _():
-            pay_in(e).wait_recv()
-
-        @pl.when((e > 0) & (e - 1 != ep))
-        def _():
-            homeward(e - 1).start()
-
-        return fold_step(state, arrived[e])
-
-    lax.fori_loop(0, experts, step, jnp.zeros(sent.shape[1:], F32))
-
-    @pl.when(ep != experts - 1)
-    def _():
-        homeward(experts - 1).start()
-
-    own_state = pltpu.make_async_copy(sent.at[ep], states.at[ep], own_sem.at[3])
-    own_state.start()
 
     for ring in weight_rings:
         ring.arrive()
@@ -600,24 +624,47 @@
         e = peer(d)
         return remote(ret_buf.at[e], back_buf.at[e], ret_send.at[d], ret_recv.at[e], "ep", e)
 
-    spray(ret_out)
+    spray(ret_out, 0, experts // 8)
+    def homeward(e):
+        return remote(
+            sent.at[e], states.at[my_head], home_send.at[e], home_recv.at[my_head], "ep", e
+        )
+
+    def home(h):
+        return remote(sent.at[0], states.at[h], home_send.at[0], home_recv.at[h], "ep", stride * h)
+
+    own_state = pltpu.make_async_copy(sent.at[ep], states.at[my_head], own_sem.at[3])
+
+    def step(e, state):
+        sent[e] = state
+
+        @pl.when(e != ep)
+        def _():
+            pay_in(e).wait_recv()
+
+        @pl.when((e > 0) & (e - 1 != ep))
+        def _():
+            homeward(e - 1).start()
+
+        return fold_step(state, arrived[e])
+
+    @pl.when(folds)
+    def _():
+        own_pay.wait()
+        lax.fori_loop(0, experts, step, jnp.zeros(sent.shape[1:], F32))
+
+        @pl.when(ep != experts - 1)
+        def _():
+            homeward(experts - 1).start()
+
+        own_state.start()
+        own_state.wait()
+
+    spray(ret_out, experts // 8, experts // 2)
     own_ret = pltpu.make_async_copy(ret_buf.at[ep], back_buf.at[ep], own_sem.at[4])
     own_ret.start()
 
-    def homecoming(d, carry):
-        home(peer(d)).wait_recv()
-        return carry
-
-    lax.fori_loop(1, experts, homecoming, 0)
-    own_state.wait()
-    for load in loads[5:7]:
-        load.wait()
-
-    def finish(pair, carry):
-        finish_mixer(pair, omap_ref, oloc_ref, states, g_ref, gain_ref, mixed_ref)
-        return carry
-
-    lax.fori_loop(0, pairs, finish, 0)
+    normed_ring.forward()
 
     class Scatter:
         def __init__(self, index, part, relay, sums):
@@ -660,27 +707,35 @@
 
     scatter_a = Scatter(0, part_a, relay_a, sums_a)
     scatter_b = Scatter(1, part_b, relay_b, sums_b)
-    mixer_rows = part_a.shape[1]
-    for s, owner in enumerate((tp, left, right, across)):
-        mine = pl.ds(pl.multiple_of(owner * mixer_rows, mixer_rows), mixer_rows)
-        part_a[s] = dot(mixed_ref[mine, :], wout_ref[...]).astype(BF16)
-    scatter_a.start()
-
-    normed_ring.forward()
+
     own_normed.wait()
     for load in loads[10:13]:
         load.wait()
     normed_ring.arrive()
-    scatter_a.forward()
     both = dot(ngather[...].reshape(tps * tokens, width), cgu_ref[...])
     inner = (jax.nn.silu(both[:, :half_lanes]) * both[:, half_lanes:]).astype(BF16)
     for s in range(4):
         part_b[s] = dot(inner[s * tokens : (s + 1) * tokens], cd_ref[...]).astype(BF16)
     scatter_b.start()
+
+    others(lambda h: home(h).wait_recv())
+    for load in loads[5:7]:
+        load.wait()
+
+    def finish(pair, carry):
+        finish_mixer(pair, omap_ref, oloc_ref, states, g_ref, gain_ref, mixed_ref)
+        return carry
+
+    lax.fori_loop(0, pairs, finish, 0)
+    mixer_rows = part_a.shape[1]
+    for s, owner in enumerate((tp, left, right, across)):
+        mine = pl.ds(pl.multiple_of(owner * mixer_rows, mixer_rows), mixer_rows)
+        part_a[s] = dot(mixed_ref[mine, :], wout_ref[...]).astype(BF16)
     scatter_b.forward()
+    scatter_a.start()
+    scatter_a.forward()
+    yacc[:tokens, :] = scatter_b.total()
     attend_ref[...] = scatter_a.total().astype(BF16)
-    moe_sum = scatter_b.total()
-    yacc[:tokens, :] = moe_sum
 
     hits, quarter = slot_hits(ids_ref[...], experts, capacity)
     own_ret.wait()
@@ -700,14 +755,17 @@
         moe_ref[:, c * quarter_width : (c + 1) * quarter_width] = block.astype(BF16)
 
     drain(outward, False)
-    drain(pay_out, False)
     drain(ret_out, False)
+    others(lambda h: pay_out(h).wait_send())
 
     def homegoing(d, carry):
         homeward(peer(d)).wait_send()
         return carry
 
-    lax.fori_loop(1, experts, homegoing, 0)
+    @pl.when(folds)
+    def _():
+        lax.fori_loop(1, experts, homegoing, 0)
+
     for item in weight_rings + (normed_ring, scatter_a, scatter_b):
         item.finish()
 
@@ -769,10 +827,10 @@
             V((shared, width), BF16),
             V((rows, mix_width), BF16),
             V((rows, mix_width), F32),
-            V((experts, 48, lanes), BF16),
-            V((experts, 48, lanes), BF16),
-            V((experts, 8, lanes), F32),
-            V((experts, 8, lanes), F32),
+            V((groups, lanes // 2, lanes), BF16),
+            V((experts, lanes // 2, lanes), BF16),
+            V((experts, lanes // 4, lanes), F32),
+            V((groups, lanes // 4, lanes), F32),
             V((rows, mix_width), BF16),
         ]
         + [V(slab, BF16)] * 4
@@ -792,7 +850,7 @@
             dma((5,)),
         ]
         + [dma((experts,))] * 8
-        + [dma((16,)), dma((16,)), dma((12,)), dma((12,))],
+        + [dma((30,)), dma((30,)), dma((12,)), dma((12,))],
         compiler_params=pltpu.CompilerParams(
             collective_id=0, has_side_effects=True, vmem_limit_bytes=62 * 1024 * 1024
         ),

time: 214 us -> 202 us (0.944)
  the two profiles are of different devices: /device:TPU:33 before, /device:TPU:808 now
where the time goes in v3:
time: 202 us
  Pallas kernels  198 us (98%)
  local copies, waits for them, and re-layouts  3.76 us (2%)
    pallas_call x1, Pallas kernels, on_device(): pl.pallas_call(functools.partial(everything, capacity), in_specs=[hbm] *...  198 us

profile of v3, /device:TPU:808, one launch (start us, length us, event | category | flops | bytes accessed | tf_op | source)
XLA Modules:
  0.0 202.3 jit_solution(8676575725741517592)
XLA Ops:
  0.6 197.8 %everything.1 = (bf16[128,2048]{1,0:T(8,128)(2,1)}, bf16[128,2048]{1,0:T(8,128)(2,1)}) custom-call(bf16[512,512]{1,0:T(8,128)(2,1)} %q_in.1, bf16[512,512]{1,0:T(8,128)(2,1)} %k_in.1, bf16[512,512]{1,0:T(8,128)(2,1)} %v_in.1, bf16[512,512]{1,0:T(8,128)(2,1)} %f_in.1, bf16[512,512]{1,0:T(8,128)(2,1)} %a_in.1, bf16[512,512]{1,0:T(8,128)(2,1)} %g_in.1, ...), custom_call_target="tpu_custom_call" | custom-call | tf_op jit(solution)/shard_map/everything/pallas_call | solution.py:812
  198.5 1.9 copy.25
  200.4 1.9 copy.26

commit v4 on v3

--- a/solution.py
+++ b/solution.py
@@ -429,7 +429,8 @@
 
         lax.fori_loop(1, experts, go, 0)
 
-    spray(outward, 0, experts // 2)
+    early = 3 * experts // 16
+    spray(outward, 0, early)
 
     class Ring:
         def __init__(self, index, own, slot, pair_left, pair_right):
@@ -559,9 +560,45 @@
     def _():
         own_pay.start()
 
+    spray(outward, early, experts // 2)
     for ring in weight_rings[1:]:
         ring.forward()
     normed_ring.start()
+
+    def homeward(e):
+        return remote(
+            sent.at[e], states.at[my_head], home_send.at[e], home_recv.at[my_head], "ep", e
+        )
+
+    def home(h):
+        return remote(sent.at[0], states.at[h], home_send.at[0], home_recv.at[h], "ep", stride * h)
+
+    own_state = pltpu.make_async_copy(sent.at[ep], states.at[my_head], own_sem.at[3])
+
+    def step(e, state):
+        sent[e] = state
+
+        @pl.when(e != ep)
+        def _():
+            pay_in(e).wait_recv()
+
+        @pl.when((e > 0) & (e - 1 != ep))
+        def _():
+            homeward(e - 1).start()
+
+        return fold_step(state, arrived[e])
+
+    @pl.when(folds)
+    def _():
+        own_pay.wait()
+        lax.fori_loop(0, experts, step, jnp.zeros(sent.shape[1:], F32))
+
+        @pl.when(ep != experts - 1)
+        def _():
+            homeward(experts - 1).start()
+
+        own_state.start()
+        own_state.wait()
 
     own_out.wait()
     drain(inward, True)
@@ -624,47 +661,9 @@
         e = peer(d)
         return remote(ret_buf.at[e], back_buf.at[e], ret_send.at[d], ret_recv.at[e], "ep", e)
 
-    spray(ret_out, 0, experts // 8)
-    def homeward(e):
-        return remote(
-            sent.at[e], states.at[my_head], home_send.at[e], home_recv.at[my_head], "ep", e
-        )
-
-    def home(h):
-        return remote(sent.at[0], states.at[h], home_send.at[0], home_recv.at[h], "ep", stride * h)
-
-    own_state = pltpu.make_async_copy(sent.at[ep], states.at[my_head], own_sem.at[3])
-
-    def step(e, state):
-        sent[e] = state
-
-        @pl.when(e != ep)
-        def _():
-            pay_in(e).wait_recv()
-
-        @pl.when((e > 0) & (e - 1 != ep))
-        def _():
-            homeward(e - 1).start()
-
-        return fold_step(state, arrived[e])
-
-    @pl.when(folds)
-    def _():
-        own_pay.wait()
-        lax.fori_loop(0, experts, step, jnp.zeros(sent.shape[1:], F32))
-
-        @pl.when(ep != experts - 1)
-        def _():
-            homeward(experts - 1).start()
-
-        own_state.start()
-        own_state.wait()
-
-    spray(ret_out, experts // 8, experts // 2)
+    spray(ret_out, 0, experts // 2)
     own_ret = pltpu.make_async_copy(ret_buf.at[ep], back_buf.at[ep], own_sem.at[4])
     own_ret.start()
-
-    normed_ring.forward()
 
     class Scatter:
         def __init__(self, index, part, relay, sums):
@@ -708,34 +707,35 @@
     scatter_a = Scatter(0, part_a, relay_a, sums_a)
     scatter_b = Scatter(1, part_b, relay_b, sums_b)
 
+    others(lambda h: home(h).wait_recv())
+    for load in loads[5:7]:
+        load.wait()
+
+    def finish(pair, carry):
+        finish_mixer(pair, omap_ref, oloc_ref, states, g_ref, gain_ref, mixed_ref)
+        return carry
+
+    lax.fori_loop(0, pairs, finish, 0)
+    mixer_rows = part_a.shape[1]
+    for s, owner in enumerate((tp, left, right, across)):
+        mine = pl.ds(pl.multiple_of(owner * mixer_rows, mixer_rows), mixer_rows)
+        part_a[s] = dot(mixed_ref[mine, :], wout_ref[...]).astype(BF16)
+    normed_ring.forward()
+    scatter_a.start()
+
     own_normed.wait()
     for load in loads[10:13]:
         load.wait()
     normed_ring.arrive()
+    scatter_a.forward()
     both = dot(ngather[...].reshape(tps * tokens, width), cgu_ref[...])
     inner = (jax.nn.silu(both[:, :half_lanes]) * both[:, half_lanes:]).astype(BF16)
     for s in range(4):
         part_b[s] = dot(inner[s * tokens : (s + 1) * tokens], cd_ref[...]).astype(BF16)
     scatter_b.start()
-
-    others(lambda h: home(h).wait_recv())
-    for load in loads[5:7]:
-        load.wait()
-
-    def finish(pair, carry):
-        finish_mixer(pair, omap_ref, oloc_ref, states, g_ref, gain_ref, mixed_ref)
-        return carry
-
-    lax.fori_loop(0, pairs, finish, 0)
-    mixer_rows = part_a.shape[1]
-    for s, owner in enumerate((tp, left, right, across)):
-        mine = pl.ds(pl.multiple_of(owner * mixer_rows, mixer_rows), mixer_rows)
-        part_a[s] = dot(mixed_ref[mine, :], wout_ref[...]).astype(BF16)
     scatter_b.forward()
-    scatter_a.start()
-    scatter_a.forward()
+    attend_ref[...] = scatter_a.total().astype(BF16)
     yacc[:tokens, :] = scatter_b.total()
-    attend_ref[...] = scatter_a.total().astype(BF16)
 
     hits, quarter = slot_hits(ids_ref[...], experts, capacity)
     own_ret.wait()
@@ -852,7 +852,7 @@
         + [dma((experts,))] * 8
         + [dma((30,)), dma((30,)), dma((12,)), dma((12,))],
         compiler_params=pltpu.CompilerParams(
-            collective_id=0, has_side_effects=True, vmem_limit_bytes=62 * 1024 * 1024
+            collective_id=0, has_side_effects=True, vmem_limit_bytes=52 * 1024 * 1024
         ),
         name="everything",
     )(

time: 202 us -> 192 us (0.950)
  the two profiles are of different devices: /device:TPU:808 before, /device:TPU:33 now
where the time goes in v4:
time: 192 us; the launch traced here: 191 us
  Pallas kernels  183 us (95%)
  local copies, waits for them, and re-layouts  7.44 us (4%)
    pallas_call x1, Pallas kernels, on_device(): pl.pallas_call(functools.partial(everything, capacity), in_specs=[hbm] *...  183 us
    unnamed x18, local copies, waits for them, and re-layouts  7.44 us

profile of v4, /device:TPU:33, one launch (start us, length us, event | category | flops | bytes accessed | tf_op | source)
XLA Modules:
  0.0 191.4 jit_solution(11271768074800671267)
XLA Ops:
  0.6 0.0 copy-start
  0.6 1.0 copy-done
  1.7 0.0 copy-start.1
  1.7 0.7 copy-done.1
  2.4 0.0 copy-start.2
  2.4 0.7 copy-done.2
  3.1 0.0 copy-start.3
  3.1 0.7 copy-done.3
  3.8 0.0 copy-start.4
  3.8 0.7 copy-done.4
  4.5 0.0 copy-start.5
  4.5 0.7 copy-done.5
  5.1 0.0 copy-start.6
  5.1 0.7 copy-done.6
  5.8 0.0 copy-start.7
  5.8 0.7 copy-done.7
  6.5 183.3 %everything.1 = (bf16[128,2048]{1,0:T(8,128)(2,1)S(1)}, bf16[128,2048]{1,0:T(8,128)(2,1)S(1)}) custom-call(bf16[512,512]{1,0:T(8,128)(2,1)S(1)} %copy-done, bf16[512,512]{1,0:T(8,128)(2,1)} %k_in.1, bf16[512,512]{1,0:T(8,128)(2,1)} %v_in.1, bf16[512,512]{1,0:T(8,128)(2,1)} %f_in.1, bf16[512,512]{1,0:T(8,128)(2,1)} %a_in.1, bf16[512,512]{1,0:T(8,128)(2,1)} %g_in.1, ...), custom_call_target="tpu_custom_call" | custom-call | tf_op jit(solution)/shard_map/everything/pallas_call | solution.py:812
  189.8 0.8 copy.25
  190.6 0.8 copy.26
Async XLA Ops:
  0.6 1.0 copy-start
  1.7 0.7 copy-start.1
  2.4 0.7 copy-start.2
  3.1 0.7 copy-start.3
  3.8 0.7 copy-start.4
  4.5 0.7 copy-start.5
  5.1 0.7 copy-start.6
  5.8 0.7 copy-start.7

commit v5 on v4

--- a/solution.py
+++ b/solution.py
@@ -197,7 +197,7 @@
     low = iota(state_ref.shape[1:], 1) < half
     tiles = []
     for h in range(2):
-        block = state_ref[2 * pair + h]
+        block = state_ref[2 * pair + h].astype(F32)
         turned = pltpu.roll(block, half, 1)
         if h == 0:
             tiles += [jnp.where(low, block, 0.0), jnp.where(low, turned, 0.0)]
@@ -242,15 +242,15 @@
     f_in,
     a_in,
     g_in,
-    fb_ref,
-    ab_ref,
-    x_ref,
-    gain_ref,
+    fb_in,
+    ab_in,
+    x_in,
+    gain_in,
     wout_in,
-    tok_ref,
-    scale_ref,
-    ids_ref,
-    mix_ref,
+    tok_in,
+    scale_in,
+    ids_in,
+    mix_in,
     gate_in,
     up_in,
     down_in,
@@ -293,6 +293,14 @@
     relay_b,
     sums_a,
     sums_b,
+    tok_ref,
+    scale_ref,
+    ids_ref,
+    fb_ref,
+    ab_ref,
+    x_ref,
+    gain_ref,
+    mix_ref,
     load_sem,
     own_sem,
     out_send,
@@ -359,10 +367,18 @@
                 (cgate_in, cgu_ref.at[:, pl.ds(0, half_lanes)]),
                 (cup_in, cgu_ref.at[:, pl.ds(half_lanes, half_lanes)]),
                 (cdown_in, cd_ref),
+                (tok_in, tok_ref),
+                (scale_in, scale_ref),
+                (ids_in, ids_ref),
+                (fb_in, fb_ref),
+                (ab_in, ab_ref),
+                (x_in, x_ref),
+                (gain_in, gain_ref),
+                (mix_in, mix_ref),
             ]
         )
     ]
-    for load in loads:
+    for load in loads[13:] + loads[:13]:
         load.start()
 
     def remote(src, dst, send, recv, axis, to):
@@ -375,6 +391,8 @@
             device_id_type=MESH,
         )
 
+    for load in loads[13:16]:
+        load.wait()
     floats = tok_ref[...].astype(F32)
     normed = (
         floats
@@ -382,7 +400,9 @@
         * scale_ref[...]
     ).astype(BF16)
     normed_own[...] = normed
-    hits, quarter = slot_hits(ids_ref[...], experts, capacity)
+    from_here = ids_ref[...] - ep
+    from_here = jnp.where(from_here < 0, from_here + experts, from_here)
+    hits, quarter = slot_hits(from_here, experts, capacity)
     stacked = jnp.concatenate(
         [normed[:, c * quarter_width : (c + 1) * quarter_width] for c in range(4)], axis=0
     )
@@ -401,12 +421,13 @@
         return lax.rem(ep + d, experts)
 
     def outward(d):
-        to = peer(d)
-        return remote(out_buf.at[to], in_buf.at[ep], out_send.at[d], out_recv.at[ep], "ep", to)
+        there = experts - d
+        return remote(
+            out_buf.at[d], in_buf.at[there], out_send.at[d], out_recv.at[there], "ep", peer(d)
+        )
 
     def inward(d):
-        e = peer(d)
-        return remote(out_buf.at[e], in_buf.at[e], out_send.at[d], out_recv.at[e], "ep", e)
+        return remote(out_buf.at[d], in_buf.at[d], out_send.at[d], out_recv.at[d], "ep", peer(d))
 
     def spray(make, first, last):
         def go(i, carry):
@@ -419,7 +440,9 @@
             make(experts // 2).start()
         lax.fori_loop(max(first, 1), last, go, 0)
 
-    def drain(make, recv):
+    far_from, far_to = (experts // 4, 3 * experts // 4)
+
+    def drain(make, recv, first=1, last=experts):
         def go(d, carry):
             if recv:
                 make(d).wait_recv()
@@ -427,7 +450,18 @@
                 make(d).wait_send()
             return carry
 
-        lax.fori_loop(1, experts, go, 0)
+        lax.fori_loop(first, last, go, 0)
+
+    def far_slots(ref, g):
+        return ref[far_from:far_to, :, g * quarter_width : (g + 1) * quarter_width].reshape(
+            8 * experts, quarter_width
+        )
+
+    def near_slots(ref, g):
+        here = slice(g * quarter_width, (g + 1) * quarter_width)
+        return jnp.concatenate([ref[:far_from, :, here], ref[far_to:, :, here]], axis=0).reshape(
+            8 * experts, quarter_width
+        )
 
     early = 3 * experts // 16
     spray(outward, 0, early)
@@ -510,12 +544,12 @@
     for ring in weight_rings:
         ring.start()
 
-    own_out = pltpu.make_async_copy(out_buf.at[ep], in_buf.at[ep], own_sem.at[0])
+    own_out = pltpu.make_async_copy(out_buf.at[0], in_buf.at[0], own_sem.at[0])
     own_out.start()
     own_normed = pltpu.make_async_copy(normed_own, ngather.at[0], own_sem.at[1])
     own_normed.start()
 
-    for load in loads[:5]:
+    for load in loads[:5] + loads[16:19]:
         load.wait()
 
     def mix(pair, carry):
@@ -576,7 +610,7 @@
     own_state = pltpu.make_async_copy(sent.at[ep], states.at[my_head], own_sem.at[3])
 
     def step(e, state):
-        sent[e] = state
+        sent[e] = state.astype(BF16)
 
         @pl.when(e != ep)
         def _():
@@ -600,43 +634,37 @@
         own_state.start()
         own_state.wait()
 
-    own_out.wait()
-    drain(inward, True)
-    block_rows = 4 * experts
-    at_row = iota((block_rows, 16 * experts), 0)
-    at_col = iota((block_rows, 16 * experts), 1)
-    for c in range(4):
-        pick = (at_col == 16 * (at_row // 4) + 4 * c + at_row % 4).astype(F32).astype(BF16)
+    half_rows = 2 * experts
+    many = groups * half_rows
+    at_row = iota((half_rows, 8 * experts), 0)
+    at_col = iota((half_rows, 8 * experts), 1)
+    picks = [
+        (at_col == 16 * (at_row // 4) + 4 * c + at_row % 4).astype(F32).astype(BF16)
+        for c in range(4)
+    ]
+
+    def unpack(slots, base):
         for g in range(groups):
-            block = in_buf[:, :, g * quarter_width : (g + 1) * quarter_width].reshape(
-                16 * experts, quarter_width
-            )
-            xbuf[
-                g * block_rows : (g + 1) * block_rows,
-                c * quarter_width : (c + 1) * quarter_width,
-            ] = dot(pick, block).astype(BF16)
-
-    for load in loads[7:10]:
-        load.wait()
-
-    def hidden(s):
-        rows = xbuf[...]
+            block = slots(in_buf, g)
+            for c in range(4):
+                xbuf[
+                    base + g * half_rows : base + (g + 1) * half_rows,
+                    c * quarter_width : (c + 1) * quarter_width,
+                ] = dot(picks[c], block).astype(BF16)
+
+    def hidden(base, s):
+        rows = xbuf[base : base + many, :]
         return (jax.nn.silu(dot(rows, wg_ref[s])) * dot(rows, wu_ref[s])).astype(BF16)
 
-    gate_ring.beside()
-    up_ring.beside()
-    for s in range(3):
-        hbuf[:, s * hid : (s + 1) * hid] = hidden(s)
-    for ring in down_rings:
-        ring.beside()
-    yacc[...] = dot(hbuf[...], wd_ref[: 3 * hid])
-
-    for ring in weight_rings:
-        ring.arrive()
-    total = yacc[...] + dot(hidden(3), wd_ref[3 * hid :])
-    yacc[...] = total
-    at_row = iota((16 * experts, block_rows), 0)
-    at_col = iota((16 * experts, block_rows), 1)
+    def lift(base):
+        for s in range(3):
+            hbuf[base : base + many, s * hid : (s + 1) * hid] = hidden(base, s)
+
+    def lower(base):
+        yacc[base : base + many, :] = dot(hbuf[base : base + many, :], wd_ref[: 3 * hid])
+
+    at_row = iota((8 * experts, half_rows), 0)
+    at_col = iota((8 * experts, half_rows), 1)
     put = jnp.concatenate(
         [
             (at_row == 16 * (at_col // 4) + 4 * c + at_col % 4).astype(F32).astype(BF16)
@@ -644,25 +672,56 @@
         ],
         axis=1,
     )
-    for g in range(groups):
-        rows = yacc[g * block_rows : (g + 1) * block_rows, :].astype(BF16)
-        rows = jnp.concatenate(
-            [rows[:, c * quarter_width : (c + 1) * quarter_width] for c in range(4)], axis=0
-        )
-        ret_buf[:, :, g * quarter_width : (g + 1) * quarter_width] = (
-            dot(put, rows).astype(BF16).reshape(experts, 16, quarter_width)
-        )
+
+    def complete(base, store):
+        total = yacc[base : base + many, :] + dot(hidden(base, 3), wd_ref[3 * hid :])
+        for g in range(groups):
+            rows = total[g * half_rows : (g + 1) * half_rows].astype(BF16)
+            rows = jnp.concatenate(
+                [rows[:, c * quarter_width : (c + 1) * quarter_width] for c in range(4)], axis=0
+            )
+            block = dot(put, rows).astype(BF16).reshape(experts // 2, 16, quarter_width)
+            store(slice(g * quarter_width, (g + 1) * quarter_width), block)
+
+    def store_far(here, block):
+        ret_buf[far_from:far_to, :, here] = block
+
+    def store_near(here, block):
+        ret_buf[:far_from, :, here] = block[:far_from]
+        ret_buf[far_to:, :, here] = block[far_from:]
 
     def ret_out(d):
-        to = peer(d)
-        return remote(ret_buf.at[to], back_buf.at[ep], ret_send.at[d], ret_recv.at[ep], "ep", to)
+        there = experts - d
+        return remote(
+            ret_buf.at[d], back_buf.at[there], ret_send.at[d], ret_recv.at[there], "ep", peer(d)
+        )
 
     def ret_in(d):
-        e = peer(d)
-        return remote(ret_buf.at[e], back_buf.at[e], ret_send.at[d], ret_recv.at[e], "ep", e)
-
-    spray(ret_out, 0, experts // 2)
-    own_ret = pltpu.make_async_copy(ret_buf.at[ep], back_buf.at[ep], own_sem.at[4])
+        return remote(ret_buf.at[d], back_buf.at[d], ret_send.at[d], ret_recv.at[d], "ep", peer(d))
+
+    drain(inward, True, far_from, far_to)
+    unpack(far_slots, 0)
+    for load in loads[7:10]:
+        load.wait()
+    gate_ring.beside()
+    up_ring.beside()
+    lift(0)
+    for ring in down_rings:
+        ring.beside()
+    lower(0)
+    own_out.wait()
+    drain(inward, True, 1, far_from)
+    drain(inward, True, far_to, experts)
+    unpack(near_slots, many)
+    lift(many)
+    lower(many)
+    for ring in weight_rings:
+        ring.arrive()
+    complete(0, store_far)
+    spray(ret_out, 0, experts // 4)
+    complete(many, store_near)
+    spray(ret_out, experts // 4, experts // 2)
+    own_ret = pltpu.make_async_copy(ret_buf.at[0], back_buf.at[0], own_sem.at[4])
     own_ret.start()
 
     class Scatter:
@@ -708,7 +767,7 @@
     scatter_b = Scatter(1, part_b, relay_b, sums_b)
 
     others(lambda h: home(h).wait_recv())
-    for load in loads[5:7]:
+    for load in loads[5:7] + loads[19:20]:
         load.wait()
 
     def finish(pair, carry):
@@ -737,22 +796,40 @@
     attend_ref[...] = scatter_a.total().astype(BF16)
     yacc[:tokens, :] = scatter_b.total()
 
-    hits, quarter = slot_hits(ids_ref[...], experts, capacity)
+    from_here = ids_ref[...] - ep
+    from_here = jnp.where(from_here < 0, from_here + experts, from_here)
+    hits, quarter = slot_hits(from_here, experts, capacity)
+    for load in loads[20:]:
+        load.wait()
+
+    def weigh(g, c):
+        weight = jnp.where(hits[g][0], mix_ref[0:1, :], 0.0) + jnp.where(
+            hits[g][1], mix_ref[1:2, :], 0.0
+        )
+        return split(jnp.where(quarter == c, weight, 0.0), 2)
+
+    far = slice(16 * far_from, 16 * far_to)
+
+    def gather(slots, take):
+        for c in range(4):
+            here = slice(c * quarter_width, (c + 1) * quarter_width)
+            block = yacc[:tokens, here]
+            for g in range(groups):
+                values = slots(back_buf, g)
+                for part in weigh(g, c):
+                    block = block + dot_tn(take(part), values)
+            yacc[:tokens, here] = block
+
+    drain(ret_in, True, far_from, far_to)
+    gather(far_slots, lambda part: part[far])
     own_ret.wait()
-    drain(ret_in, True)
-    for c in range(4):
-        block = yacc[:tokens, c * quarter_width : (c + 1) * quarter_width]
-        for g in range(groups):
-            weight = jnp.where(hits[g][0], mix_ref[0:1, :], 0.0) + jnp.where(
-                hits[g][1], mix_ref[1:2, :], 0.0
-            )
-            weight = jnp.where(quarter == c, weight, 0.0)
-            values = back_buf[:, :, g * quarter_width : (g + 1) * quarter_width].reshape(
-                16 * experts, quarter_width
-            )
-            for part in split(weight, 2):
-                block = block + dot_tn(part, values)
-        moe_ref[:, c * quarter_width : (c + 1) * quarter_width] = block.astype(BF16)
+    drain(ret_in, True, 1, far_from)
+    drain(ret_in, True, far_to, experts)
+    gather(
+        near_slots,
+        lambda part: jnp.concatenate([part[: far.start], part[far.stop :]], axis=0),
+    )
+    moe_ref[...] = yacc[:tokens, :].astype(BF16)
 
     drain(outward, False)
     drain(ret_out, False)
@@ -805,13 +882,13 @@
     shared = common_switch_matrix.shape[1]
     slab = (experts, 16, capacity * width // 16)
     vmem = pl.BlockSpec(memory_space=pltpu.VMEM)
-    hbm = pl.BlockSpec(memory_space=pl.ANY)
+    hbm = pl.BlockSpec(memory_space=pltpu.HBM)
     V = pltpu.VMEM
     dma = pltpu.SemaphoreType.DMA
     mixer_rows = rows // tps
     return pl.pallas_call(
         functools.partial(everything, capacity),
-        in_specs=[hbm] * 6 + [vmem] * 4 + [hbm] + [vmem] * 4 + [hbm] * 6,
+        in_specs=[hbm] * 21,
         out_specs=(vmem, vmem),
         out_shape=(
             jax.ShapeDtypeStruct((mixer_rows, width), BF16),
@@ -829,8 +906,8 @@
             V((rows, mix_width), F32),
             V((groups, lanes // 2, lanes), BF16),
             V((experts, lanes // 2, lanes), BF16),
-            V((experts, lanes // 4, lanes), F32),
-            V((groups, lanes // 4, lanes), F32),
+            V((experts, lanes // 4, lanes), BF16),
+            V((groups, lanes // 4, lanes), BF16),
             V((rows, mix_width), BF16),
         ]
         + [V(slab, BF16)] * 4
@@ -846,13 +923,21 @@
             V((2, tokens // 2, width), BF16),
             V((tps, mixer_rows, width), BF16),
             V((tps, tokens, width), BF16),
-            dma((13,)),
+            V((tokens, width), BF16),
+            V((1, width), F32),
+            V((top_count, tokens), jnp.int32),
+            V((1, mix_width), F32),
+            V((1, mix_width), F32),
+            V((groups, rows), F32),
+            V((1, mix_width), F32),
+            V((top_count, tokens), F32),
+            dma((21,)),
             dma((5,)),
         ]
         + [dma((experts,))] * 8
         + [dma((30,)), dma((30,)), dma((12,)), dma((12,))],
         compiler_params=pltpu.CompilerParams(
-            collective_id=0, has_side_effects=True, vmem_limit_bytes=52 * 1024 * 1024
+            collective_id=0, has_side_effects=True, vmem_limit_bytes=60 * 1024 * 1024
         ),
         name="everything",
     )(

time: 192 us -> 184 us (0.958)
  Pallas kernels: 183 us -> 179 us
  local copies, waits for them, and re-layouts: 7.44 us -> 3.76 us
    pallas_call x1, Pallas kernels: 183 us -> 179 us  [on_device(): pl.pallas_call(functools.partial(everything, capacity), in_specs=[hbm] *...]
    unnamed x18 -> x2, local copies, waits for them, and re-layouts: 7.44 us -> 3.76 us
where the time goes in v5:
time: 184 us
  Pallas kernels  179 us (97%)
  local copies, waits for them, and re-layouts  3.76 us (2%)
    pallas_call x1, Pallas kernels, on_device(): pl.pallas_call(functools.partial(everything, capacity), in_specs=[hbm] *...  179 us
    unnamed x2, local copies, waits for them, and re-layouts  3.76 us

profile of v5, /device:TPU:33, one launch (start us, length us, event | category | flops | bytes accessed | tf_op | source)
XLA Modules:
  0.0 183.7 jit_solution(8194709821718227499)
XLA Ops:
  0.6 179.3 %everything.1 = (bf16[128,2048]{1,0:T(8,128)(2,1)}, bf16[128,2048]{1,0:T(8,128)(2,1)}) custom-call(bf16[512,512]{1,0:T(8,128)(2,1)} %q_in.1, bf16[512,512]{1,0:T(8,128)(2,1)} %k_in.1, bf16[512,512]{1,0:T(8,128)(2,1)} %v_in.1, bf16[512,512]{1,0:T(8,128)(2,1)} %f_in.1, bf16[512,512]{1,0:T(8,128)(2,1)} %a_in.1, bf16[512,512]{1,0:T(8,128)(2,1)} %g_in.1, ...), custom_call_target="tpu_custom_call" | custom-call | tf_op jit(solution)/shard_map/everything/pallas_call | solution.py:889
  180.0 1.9 %copy.25 = bf16[128,2048]{1,0:T(8,128)(2,1)} copy(bf16[128,2048]{1,0:T(8,128)(2,1)} %get-tuple-element.4) | data formatting | bytes 1048576
  181.8 1.9 %copy.26 = bf16[128,2048]{1,0:T(8,128)(2,1)} copy(bf16[128,2048]{1,0:T(8,128)(2,1)} %get-tuple-element.5) | data formatting | bytes 1048576

commit v6 on v5

--- a/solution.py
+++ b/solution.py
@@ -709,16 +709,16 @@
     for ring in down_rings:
         ring.beside()
     lower(0)
+    for ring in weight_rings:
+        ring.arrive()
+    complete(0, store_far)
+    spray(ret_out, 0, experts // 4)
     own_out.wait()
     drain(inward, True, 1, far_from)
     drain(inward, True, far_to, experts)
     unpack(near_slots, many)
     lift(many)
     lower(many)
-    for ring in weight_rings:
-        ring.arrive()
-    complete(0, store_far)
-    spray(ret_out, 0, experts // 4)
     complete(many, store_near)
     spray(ret_out, experts // 4, experts // 2)
     own_ret = pltpu.make_async_copy(ret_buf.at[0], back_buf.at[0], own_sem.at[4])
@@ -845,6 +845,28 @@
 
     for item in weight_rings + (normed_ring, scatter_a, scatter_b):
         item.finish()
+
+
+def emit(a_in, b_in, a_out, b_out, buf, in_sem, out_sem):
+    half = a_in.shape[0] // 2
+    moves = []
+    for i, (src, dst) in enumerate([(a_in, a_out), (b_in, b_out)]):
+        for j in range(2):
+            n = 2 * i + j
+            at = pl.ds(j * half, half)
+            moves.append(
+                (
+                    pltpu.make_async_copy(src.at[at], buf.at[n], in_sem.at[n]),
+                    pltpu.make_async_copy(buf.at[n], dst.at[at], out_sem.at[n]),
+                )
+            )
+    for load, _ in moves:
+        load.start()
+    for load, store in moves:
+        load.wait()
+        store.start()
+    for _, store in moves:
+        store.wait()
 
 
 def on_device(
@@ -886,7 +908,7 @@
     V = pltpu.VMEM
     dma = pltpu.SemaphoreType.DMA
     mixer_rows = rows // tps
-    return pl.pallas_call(
+    attend, moe = pl.pallas_call(
         functools.partial(everything, capacity),
         in_specs=[hbm] * 21,
         out_specs=(vmem, vmem),
@@ -963,6 +985,18 @@
         common_raising_matrix,
         common_lowering_matrix,
     )
+    return pl.pallas_call(
+        emit,
+        in_specs=[hbm, hbm],
+        out_specs=(hbm, hbm),
+        out_shape=(
+            jax.ShapeDtypeStruct(attend.shape, BF16),
+            jax.ShapeDtypeStruct(moe.shape, BF16),
+        ),
+        scratch_shapes=[V((4, tokens // 2, width), BF16), dma((4,)), dma((4,))],
+        compiler_params=pltpu.CompilerParams(vmem_limit_bytes=60 * 1024 * 1024),
+        name="emit",
+    )(attend, moe)
 
 
 def solution(mesh):

time: 184 us -> 181 us (0.984)
  local copies, waits for them, and re-layouts: 3.76 us -> 0 us
    unnamed x2 -> x0, local copies, waits for them, and re-layouts: 3.76 us -> none
    pallas_call x0 -> x1, Pallas kernels: none -> 1.98 us  [on_device(): pl.pallas_call(emit, in_specs=[hbm, hbm], out_specs=(hbm, hbm), out_shape...]
where the time goes in v6:
time: 181 us
  Pallas kernels  180 us (99%)
    pallas_call x1, Pallas kernels, on_device(): pl.pallas_call(functools.partial(everything, capacity), in_specs=[hbm] *...  178 us

profile of v6, /device:TPU:33, one launch (start us, length us, event | category | flops | bytes accessed | tf_op | source)
XLA Modules:
  0.0 180.5 jit_solution(10457773118458863297)
XLA Ops:
  0.6 177.7 %everything.1 = (bf16[128,2048]{1,0:T(8,128)(2,1)}, bf16[128,2048]{1,0:T(8,128)(2,1)}) custom-call(bf16[512,512]{1,0:T(8,128)(2,1)} %q_in.1, bf16[512,512]{1,0:T(8,128)(2,1)} %k_in.1, bf16[512,512]{1,0:T(8,128)(2,1)} %v_in.1, bf16[512,512]{1,0:T(8,128)(2,1)} %f_in.1, bf16[512,512]{1,0:T(8,128)(2,1)} %a_in.1, bf16[512,512]{1,0:T(8,128)(2,1)} %g_in.1, ...), custom_call_target="tpu_custom_call" | custom-call | tf_op jit(solution)/shard_map/everything/pallas_call | solution.py:911
  178.4 2.0 %emit.1 = (bf16[128,2048]{1,0:T(8,128)(2,1)}, bf16[128,2048]{1,0:T(8,128)(2,1)}) custom-call(bf16[128,2048]{1,0:T(8,128)(2,1)} %get-tuple-element.4.a_in, bf16[128,2048]{1,0:T(8,128)(2,1)} %get-tuple-element.5.b_in), custom_call_target="tpu_custom_call" | custom-call | tf_op jit(solution)/shard_map/emit/pallas_call | solution.py:988

commit v7 on v6

--- a/solution.py
+++ b/solution.py
@@ -553,7 +553,7 @@
         load.wait()
 
     def mix(pair, carry):
-        @pl.when(pair == pairs // 2)
+        @pl.when(pair == pairs // 4)
         def _():
             gate_ring.forward()
 

time: 181 us -> 181 us (level)
  no operation moved by 1% of the time
where the time goes in v7:
time: 181 us; the launch traced here: 180 us
  Pallas kernels  180 us (99%)
    pallas_call x1, Pallas kernels, on_device(): pl.pallas_call(functools.partial(everything, capacity), in_specs=[hbm] *...  178 us

profile of v7, /device:TPU:33, one launch (start us, length us, event | category | flops | bytes accessed | tf_op | source)
XLA Modules:
  0.0 180.5 jit_solution(2268594809109998517)
XLA Ops:
  0.6 177.7 %everything.1 = (bf16[128,2048]{1,0:T(8,128)(2,1)}, bf16[128,2048]{1,0:T(8,128)(2,1)}) custom-call(bf16[512,512]{1,0:T(8,128)(2,1)} %q_in.1, bf16[512,512]{1,0:T(8,128)(2,1)} %k_in.1, bf16[512,512]{1,0:T(8,128)(2,1)} %v_in.1, bf16[512,512]{1,0:T(8,128)(2,1)} %f_in.1, bf16[512,512]{1,0:T(8,128)(2,1)} %a_in.1, bf16[512,512]{1,0:T(8,128)(2,1)} %g_in.1, ...), custom_call_target="tpu_custom_call" | custom-call | tf_op jit(solution)/shard_map/everything/pallas_call | solution.py:911
  178.3 2.0 %emit.1 = (bf16[128,2048]{1,0:T(8,128)(2,1)}, bf16[128,2048]{1,0:T(8,128)(2,1)}) custom-call(bf16[128,2048]{1,0:T(8,128)(2,1)} %get-tuple-element.4.a_in, bf16[128,2048]{1,0:T(8,128)(2,1)} %get-tuple-element.5.b_in), custom_call_target="tpu_custom_call" | custom-call | tf_op jit(solution)/shard_map/emit/pallas_call | solution.py:988
